TPU v7x, 512 devices: a whole 4x8x8 slice. The times are simulated.
512 devices in a mesh: ep: 32 (over z, x), tp: 16 (over y, core).
Axes of the slice: x: 4, y: 8, z: 8, core: 2. Of those that a mesh axis runs over, the one named last changes fastest.
Arguments:
- queries: bfloat16 [16384, 2048], P('ep', 'tp'), may hold values from -6 to 6
- keys: bfloat16 [16384, 2048], P('ep', 'tp'), may hold values from -12 to 12
- values: bfloat16 [16384, 2048], P('ep', 'tp'), may hold values from -8 to 8
- key_bias: bfloat16 [16384, 16], P('ep', 'tp'), may hold values from -16 to 0
- out_weight: bfloat16 [2048, 2048], P('tp'), may hold values from -0.1875 to 0.1875
- moe_input: bfloat16 [4096, 2048], P('ep'), may hold values from -6 to 6
- moe_gain: float32 [2048], replicated, may hold values from 0.1 to 1.9
- route_ids: int32 [4096, 2], P('ep'), may hold values from 0 to 31, all different within a row; in each aligned block of 128 rows (0 to 127, 128 to 255, ...) at most 12 rows name the same one
- route_scores: float32 [4096, 2], P('ep'), may hold values from 0.05 to 1
- shared_gate: bfloat16 [2048, 2048], P(None, 'tp'), may hold values from -0.125 to 0.125
- shared_up: bfloat16 [2048, 2048], P(None, 'tp'), may hold values from -0.125 to 0.125
- shared_down: bfloat16 [2048, 2048], P('tp'), may hold values from -0.1875 to 0.1875
- expert_gate: bfloat16 [32, 2048, 2048], P('ep', None, 'tp'), may hold values from -0.125 to 0.125
- expert_up: bfloat16 [32, 2048, 2048], P('ep', None, 'tp'), may hold values from -0.125 to 0.125
- expert_down: bfloat16 [32, 2048, 2048], P('ep', 'tp'), may hold values from -0.1875 to 0.1875
Outputs:
- mixed_tokens: bfloat16 [16384, 2048], P('ep', 'tp')
- expert_mix: bfloat16 [4096, 2048], P('ep', 'tp')
Inputs may be any that keep to these rules, and one draw needn't show every extreme that they name: `route_ids`: each row names 2 different experts. Among the 128 rows of one index of ep no expert is named by more than 12 rows, and in some such block one expert is named by exactly 12 rows.
All inputs are finite; a program needn't handle non-finite values.
Results may differ from a plain program's by a relative error of at most 0.019.
Values may be sent and summed in bfloat16 or wider, within the bound.
A program may use at most 128 MiB of HBM per device.

v0:
```python
import jax
import jax.numpy as jnp
from jax import lax
from jax.sharding import PartitionSpec as P

SEQUENCE_COUNT = 1


EPS_NORM = 1e-06
ROUTED_SCALE = 2.5


def sent_together(arrays, axis, dim, along):
    both = jnp.concatenate(arrays, axis=along)
    filled, at, done = (lax.all_gather(both, axis, axis=dim, tiled=True), 0, [])
    for a in arrays:
        done.append(lax.slice_in_dim(filled, at, at + a.shape[along], axis=along))
        at += a.shape[along]
    return tuple(done)


def laid_out(blocks, dim):
    blocks = jnp.moveaxis(blocks, 0, dim)
    shape = blocks.shape
    return blocks.reshape(*shape[:dim], shape[dim] * shape[dim + 1], *shape[dim + 2 :])


def from_everyone(array, axis):
    count = lax.axis_size(axis)
    return lax.all_to_all(
        jnp.broadcast_to(array[None], (count, *array.shape)), axis, 0, 0, tiled=True
    )


def gathered_copies(array, axis, dim):
    return laid_out(from_everyone(array, axis), dim)


def absorb(state, query_heads, piece, visible):
    total, carried = state
    key_piece, value_piece, bias_piece = piece
    span = key_piece.shape[0]
    heads = query_heads.shape[1]
    key_heads = key_piece.reshape(span, heads, -1)
    value_heads = value_piece.reshape(span, heads, -1)
    scale = query_heads.shape[2] ** (-0.5)
    logit = (
        jnp.einsum("qhd,khd->hqk", query_heads, key_heads, preferred_element_type=jnp.float32)
        * scale
    )
    logit = logit + bias_piece.astype(jnp.float32).T[:, None, :]
    keep = jnp.where(visible[None], jax.nn.log_sigmoid(-logit), 0.0)
    stay = lax.cumsum(keep, axis=2, reverse=True) - keep + carried[:, :, None]
    weight = jnp.where(visible[None], jnp.exp(jax.nn.log_sigmoid(logit) + stay), 0.0).astype(
        jnp.bfloat16
    )
    total = total + jnp.einsum(
        "hqk,khd->qhd", weight, value_heads, preferred_element_type=jnp.float32
    )
    return (total, carried + jnp.sum(keep, axis=2))


def fresh_state(query_heads):
    return (
        jnp.zeros(query_heads.shape, jnp.float32),
        jnp.zeros((query_heads.shape[1], query_heads.shape[0]), jnp.float32),
    )


def diagonal(query_heads, piece):
    count = query_heads.shape[0]
    span = piece[0].shape[0]
    key_pos = jnp.arange(span, dtype=jnp.int32)
    query_pos = jnp.arange(count, dtype=jnp.int32)
    visible = key_pos[None, :] < query_pos[:, None]
    return absorb(fresh_state(query_heads), query_heads, piece, visible)


def body(
    queries,
    keys,
    values,
    key_bias,
    out_weight,
    moe_input,
    moe_gain,
    route_ids,
    route_scores,
    shared_gate,
    shared_up,
    shared_down,
    expert_gate,
    expert_up,
    expert_down,
):
    span = queries.shape[0]
    heads = key_bias.shape[1]
    query_heads = queries.reshape(span, heads, -1)
    ep_count = lax.axis_size("ep")
    seq_devices = ep_count // SEQUENCE_COUNT
    own_index = lax.axis_index("ep")
    place = own_index % seq_devices
    own_piece = (keys, values, key_bias)
    everything = jnp.ones((span, span), jnp.bool_)
    whole = sent_together((own_piece[0], own_piece[1], own_piece[2]), "ep", 0, 1)

    def visit_gathered(turn, current):
        source = jnp.maximum(own_index - turn, 0)
        piece = tuple(
            (lax.dynamic_slice_in_dim(member, source * span, span, 0) for member in whole)
        )

        def taken(inner):
            return absorb(inner, query_heads, piece, everything)

        def skipped(inner):
            return inner

        return lax.cond(place >= turn, taken, skipped, current)

    state = lax.fori_loop(1, seq_devices, visit_gathered, diagonal(query_heads, own_piece))
    heads_out = state[0].astype(jnp.bfloat16).reshape(span, -1)
    col_count = out_weight.shape[1] // lax.axis_size("tp")
    token_count = moe_input.shape[0]
    inputs = moe_input.astype(jnp.float32)
    normed = (
        inputs * lax.rsqrt(jnp.mean(inputs * inputs, axis=-1, keepdims=True) + EPS_NORM) * moe_gain
    ).astype(jnp.bfloat16)
    own_cols = lax.dynamic_slice_in_dim(normed, lax.axis_index("tp") * col_count, col_count, 1)
    shared_hidden = (
        jax.nn.silu(jnp.dot(normed, shared_gate, preferred_element_type=jnp.float32))
        * jnp.dot(normed, shared_up, preferred_element_type=jnp.float32)
    ).astype(jnp.bfloat16)
    local_experts = expert_gate.shape[0]
    expert_count = local_experts * ep_count
    topk = route_ids.shape[1]
    capacity = 3 * token_count * topk // (2 * expert_count)
    chosen = route_ids.reshape(-1)
    onehot = (chosen[:, None] == jnp.arange(expert_count, dtype=jnp.int32)[None, :]).astype(
        jnp.int32
    )
    place_in = jnp.sum((jnp.cumsum(onehot, axis=0) - onehot) * onehot, axis=1)
    slot_ids = chosen * capacity + place_in
    send_slots = expert_count * capacity
    matches = (
        slot_ids.reshape(token_count, topk)[None]
        == jnp.arange(send_slots, dtype=jnp.int32)[:, None, None]
    )
    dispatch = jnp.sum(matches.astype(jnp.bfloat16), axis=2)
    outgoing = jnp.dot(dispatch, own_cols, preferred_element_type=jnp.float32).astype(jnp.bfloat16)
    arrived = lax.all_to_all(outgoing, "ep", split_axis=0, concat_axis=0, tiled=True)
    piece = gathered_copies(arrived, "tp", 1)
    width = piece.shape[1]
    grid = piece.reshape(ep_count, local_experts, capacity, width)
    gate_sum = jnp.einsum("secd,edf->secf", grid, expert_gate, preferred_element_type=jnp.float32)
    up_sum = jnp.einsum("secd,edf->secf", grid, expert_up, preferred_element_type=jnp.float32)
    expert_hidden = (jax.nn.silu(gate_sum) * up_sum).astype(jnp.bfloat16)
    routed = jnp.einsum(
        "secf,efd->dsec", expert_hidden, expert_down, preferred_element_type=jnp.float32
    ).reshape(lax.axis_size("tp") * col_count, -1)
    common = jnp.einsum("tf,fd->dt", shared_hidden, shared_down, preferred_element_type=jnp.float32)
    summed = lax.psum_scatter(
        jnp.concatenate(
            [
                jnp.einsum("rh,hd->dr", heads_out, out_weight, preferred_element_type=jnp.float32),
                jnp.concatenate([routed, common], axis=1),
            ],
            axis=1,
        ).astype(jnp.bfloat16),
        "tp",
        scatter_dimension=0,
        tiled=True,
    ).astype(jnp.float32)
    mixer_sum = summed[:, :span]
    expert_sum = summed[:, span:]
    mixed_tokens = mixer_sum.T.astype(jnp.bfloat16)
    routed_sum = expert_sum[:, :send_slots].astype(jnp.bfloat16)
    common_sum = expert_sum[:, send_slots:]
    returned = lax.all_to_all(routed_sum, "ep", split_axis=1, concat_axis=1, tiled=True)
    picked = (
        jnp.take(returned, slot_ids, axis=1)
        .astype(jnp.float32)
        .reshape(col_count, token_count, topk)
    )
    gates = route_scores / jnp.sum(route_scores, axis=-1, keepdims=True) * ROUTED_SCALE
    expert_mix = (common_sum + jnp.sum(picked * gates[None], axis=2)).T.astype(jnp.bfloat16)
    return (mixed_tokens, expert_mix)


def solution(mesh):
    return jax.shard_map(
        body,
        mesh=mesh,
        in_specs=(
            P("ep", "tp"),
            P("ep", "tp"),
            P("ep", "tp"),
            P("ep", "tp"),
            P("tp", None),
            P("ep", None),
            P(),
            P("ep", None),
            P("ep", None),
            P(None, "tp"),
            P(None, "tp"),
            P("tp", None),
            P("ep", None, "tp"),
            P("ep", None, "tp"),
            P("ep", "tp", None),
        ),
        out_specs=(P("ep", "tp"), P("ep", "tp")),
        check_vma=False,
    )
```

profile of v0, /device:TPU:6, one launch (start us, length us, event | category | flops | bytes accessed | tf_op | source)
XLA Modules:
  0.0 553.0 jit_solution(18031747688468072209)
XLA Ops:
  7.2 1.1 copy.87
  8.3 1.0 copy.88
  9.3 1.4 pad_maximum_fusion.1
  13.8 1.2 fusion.27
  15.0 1.2 fusion.29
  16.5 22.2 %all_to_all.26 = bf16[32,12,128]{2,1,0:T(8,128)(2,1)S(1)} all-to-all(bf16[32,12,128]{2,1,0:T(8,128)(2,1)S(1)} %all_to_all.17), channel_id=1, replica_groups=mesh['ep'=32,'tp'=16] {'ep'}, dimensions={0} | all-to-all | bytes 196608 | tf_op jit(solution)/shard_map/all_to_all | solution.py:151
  38.7 1.5 broadcast_in_dim.18
  40.2 7.1 %all-to-all-start.1 = ((bf16[16,384,128]{2,1,0:T(8,128)(2,1)}), bf16[16,384,128]{2,1,0:T(8,128)(2,1)S(1)}, u32[]{:S(2)}, u32[]{:S(2)}) async-start(bf16[16,384,128]{2,1,0:T(8,128)(2,1)} %broadcast_in_dim.18), calls=%async_computation.1 | async-start | bytes 3145728 | tf_op jit(solution)/shard_map/all_to_all | solution.py:30
  47.4 2.5 fusion.62
  50.0 4.8 fusion.38
  54.8 1.0 copy-done.1
  55.8 1.3 copy.86
  57.8 2.5 fusion.34
  60.6 0.9 fusion.65
  61.5 1.8 fusion.20
  63.3 21.9 %all-to-all-done.1 = bf16[16,384,128]{2,1,0:T(8,128)(2,1)S(1)} async-done(((bf16[16,384,128]{2,1,0:T(8,128)(2,1)}), bf16[16,384,128]{2,1,0:T(8,128)(2,1)S(1)}, u32[]{:S(2)}, u32[]{:S(2)}) %all-to-all-start.1) | async-done | bytes 1572896 | tf_op jit(solution)/shard_map/all_to_all | solution.py:30
  85.2 2.2 copy.96
  87.4 2.9 reshape.313
  90.3 2.2 convolution_bitcast_fusion.3
  92.5 2.2 fusion.23
  94.8 2.8 fusion.19
  97.6 27.0 %all-gather.2.cloned.1.call-done = bf16[16384,257]{0,1:T(8,128)(2,1)} async-done(((bf16[512,257]{0,1:T(8,128)(2,1)}), bf16[16384,257]{0,1:T(8,128)(2,1)}) %all-gather.2.cloned.1.call-update) | async-done | bytes 8421392 | tf_op jit(solution)/shard_map/all_gather | solution.py:15
  124.6 5.8 %fusion.64 = (bf16[16384,128]{0,1:T(8,128)(2,1)}, bf16[16384,128]{0,1:T(8,128)(2,1)}) fusion(bf16[16384,257]{0,1:T(8,128)(2,1)} %all-gather.2.cloned.1.call-done), kind=kLoop, calls=%fused_computation.107 | loop fusion | bytes 16777216 | tf_op jit(solution)/shard_map/slice | solution.py:17
  130.5 6.4 %copy.91 = bf16[16384,128]{1,0:T(8,128)(2,1)} copy(bf16[16384,128]{0,1:T(8,128)(2,1)} %get-tuple-element.368) | data formatting | bytes 8388608 | tf_op jit(solution)/shard_map/while | solution.py:121
  136.8 6.4 %copy.90 = bf16[16384,128]{1,0:T(8,128)(2,1)} copy(bf16[16384,128]{0,1:T(8,128)(2,1)} %get-tuple-element.369) | data formatting | bytes 8388608 | tf_op jit(solution)/shard_map/while | solution.py:121
  143.2 1.0 slice.73
  144.2 30.5 %while.15 = (s32[]{:T(128)}, f32[512,1,128]{0,2,1:T(8,128)S(1)}, f32[1,512]{1,0:T(1,128)S(1)}, s32[]{:T(128)}, s32[]{:T(128)}, /*index=5*/bf16[16384,128]{1,0:T(...) while((s32[]{:T(128)}, f32[512,1,128]{0,2,1:T(8,128)S(1)}, ...), condition=%wide.region_9.10_spmd, body=%wide.region_3.0_spmd.sunk | while | flops 175448576 | bytes 10433841 | solution.py:121
  144.2 9.7 %conditional.2 = ((f32[512,1,128]{0,2,1:T(8,128)S(1)}, f32[1,512]{1,0:T(1,128)S(1)})) conditional(s32[]{:T(128)} %convert_element_type.118, (f32[512,1,128]{0,2,1:T(8,128)S(1)}, f32[1,512]{1,0:T(1,128)S(1)}) %tuple.67, (s32[]{:T(128)}, s32[]{:T(128)}, bf16[16384,128]{1,0:T(8,128)(2,1)}, bf16[16384,128]{1,0:T(8,128)(2,1)}, ...), branch_computations={%region_4.4_spmd, %region_5.8_spmd} | conditional | flops 175448576 | bytes 10433646 | solution.py:119
  144.3 1.8 fusion.11
  146.1 4.8 fusion.9
  151.3 1.4 fusion.6
  152.7 1.2 fusion.2
  154.0 9.7 %conditional.2 = ((f32[512,1,128]{0,2,1:T(8,128)S(1)}, f32[1,512]{1,0:T(1,128)S(1)})) conditional(s32[]{:T(128)} %convert_element_type.118, (f32[512,1,128]{0,2,1:T(8,128)S(1)}, f32[1,512]{1,0:T(1,128)S(1)}) %tuple.67, (s32[]{:T(128)}, s32[]{:T(128)}, bf16[16384,128]{1,0:T(8,128)(2,1)}, bf16[16384,128]{1,0:T(8,128)(2,1)}, ...), branch_computations={%region_4.4_spmd, %region_5.8_spmd} | conditional | flops 175448576 | bytes 10433646 | solution.py:119
  154.0 1.8 fusion.11
  155.9 4.8 fusion.9
  161.1 1.4 fusion.6
  162.5 1.2 fusion.2
  163.7 9.7 %conditional.2 = ((f32[512,1,128]{0,2,1:T(8,128)S(1)}, f32[1,512]{1,0:T(1,128)S(1)})) conditional(s32[]{:T(128)} %convert_element_type.118, (f32[512,1,128]{0,2,1:T(8,128)S(1)}, f32[1,512]{1,0:T(1,128)S(1)}) %tuple.67, (s32[]{:T(128)}, s32[]{:T(128)}, bf16[16384,128]{1,0:T(8,128)(2,1)}, bf16[16384,128]{1,0:T(8,128)(2,1)}, ...), branch_computations={%region_4.4_spmd, %region_5.8_spmd} | conditional | flops 175448576 | bytes 10433646 | solution.py:119
  163.7 1.8 fusion.11
  165.6 4.8 fusion.9
  170.8 1.4 fusion.6
  172.2 1.2 fusion.2
  175.5 6.7 %pad_maximum_fusion = bf16[2048,1024]{0,1:T(8,128)(2,1)} fusion(bf16[2048,128]{0,1:T(8,128)(2,1)S(1)} %fusion.20, bf16[2048,384]{0,1:T(8,128)(2,1)} %fusion.19, bf16[2048,512]{0,1:T(8,128)(2,1)S(1)} %fusion.18), kind=kLoop, calls=%fused_computation.27 | loop fusion | flops 12582912 | bytes 8388608 | tf_op jit(solution)/shard_map/concatenate | solution.py:163
  182.2 6.4 %copy.103 = bf16[2048,1024]{1,0:T(8,128)(2,1)} copy(bf16[2048,1024]{0,1:T(8,128)(2,1)} %pad_maximum_fusion) | data formatting | bytes 8388608
  189.6 333.4 %reduce-scatter.4.cloned.1.call-done = bf16[128,1024]{1,0:T(8,128)(2,1)} async-done(((bf16[2048,1024]{1,0:T(8,128)(2,1)}), bf16[128,1024]{1,0:T(8,128)(2,1)}) %reduce-scatter.4.cloned.1.call-update) | async-done | bytes 262160
  524.7 10.7 %all-to-all-start.2 = ((bf16[128,32,12]{0,2,1:T(8,128)(2,1)}), bf16[128,32,12]{0,2,1:T(8,128)(2,1)S(1)}, u32[]{:S(2)}, u32[]{:S(2)}) async-start(bf16[128,32,12]{0,2,1:T(8,128)(2,1)} %all_to_all.20), calls=%async_computation.2 | async-start | bytes 262144 | tf_op jit(solution)/shard_map/all_to_all | solution.py:179
  536.5 0.9 slice.75
  538.2 6.0 %all-to-all-done.2 = bf16[128,32,12]{0,2,1:T(8,128)(2,1)S(1)} async-done(((bf16[128,32,12]{0,2,1:T(8,128)(2,1)}), bf16[128,32,12]{0,2,1:T(8,128)(2,1)S(1)}, u32[]{:S(2)}, u32[]{:S(2)}) %all-to-all-start.2) | async-done | bytes 98336 | tf_op jit(solution)/shard_map/all_to_all | solution.py:179
  (112 shorter events, 13.1 us)
Async XLA Ops:
  7.2 167.6 %copy-start = (bf16[128,2048]{1,0:T(8,128)(2,1)S(1)}, bf16[128,2048]{1,0:T(8,128)(2,1)}, u32[]{:S(2)}) copy-start(bf16[128,2048]{1,0:T(8,128)(2,1)} %param.23) | copy-start | bytes 1572868
  7.2 117.4 %all-gather.2.cloned.1.call-start = ((), (), s32[]{:S(2)}) async-start(), calls=%async_computation.4 | async-start | bytes 8921088 | tf_op jit(solution)/shard_map/all_gather | solution.py:15
  10.7 36.7 %copy-start.6 = (bf16[512,1]{0,1:T(2,128)(2,1)S(1)}, bf16[512,1]{0,1:T(2,128)(2,1)}, u32[]{:S(2)}) copy-start(bf16[512,1]{0,1:T(2,128)(2,1)} %param.22) | copy-start | bytes 3076
  10.7 36.7 %copy-start.4 = (bf16[512,128]{1,0:T(8,128)(2,1)S(1)}, bf16[512,128]{1,0:T(8,128)(2,1)}, u32[]{:S(2)}) copy-start(bf16[512,128]{1,0:T(8,128)(2,1)} %param.20) | copy-start | bytes 393220
  40.2 45.0 %all-to-all-start.1 = ((bf16[16,384,128]{2,1,0:T(8,128)(2,1)}), bf16[16,384,128]{2,1,0:T(8,128)(2,1)S(1)}, u32[]{:S(2)}, u32[]{:S(2)}) async-start(bf16[16,384,128]{2,1,0:T(8,128)(2,1)} %broadcast_in_dim.18), calls=%async_computation.1 | async-start | bytes 3145728 | tf_op jit(solution)/shard_map/all_to_all | solution.py:30
  47.3 475.6 %reduce-scatter.4.cloned.1.call-start = ((), (), s32[]{:S(2)}) async-start(), calls=%async_computation.5 | async-start | bytes 4456448
  50.0 10.3 %copy-start.2 = (bf16[512,128]{1,0:T(8,128)(2,1)S(1)}, bf16[512,128]{1,0:T(8,128)(2,1)}, u32[]{:S(2)}) copy-start(bf16[512,128]{1,0:T(8,128)(2,1)} %param.21) | copy-start | bytes 393220
  50.0 10.6 %copy-start.3 = (bf16[2048,128]{1,0:T(8,128)(2,1)S(1)}, bf16[2048,128]{1,0:T(8,128)(2,1)}, u32[]{:S(2)}) copy-start(bf16[2048,128]{1,0:T(8,128)(2,1)} %param.28) | copy-start | bytes 1572868
  54.8 1.0 copy-start.1
  188.6 0.7 copy-start.7
  188.6 0.7 copy-start.5
  524.7 19.6 %all-to-all-start.2 = ((bf16[128,32,12]{0,2,1:T(8,128)(2,1)}), bf16[128,32,12]{0,2,1:T(8,128)(2,1)S(1)}, u32[]{:S(2)}, u32[]{:S(2)}) async-start(bf16[128,32,12]{0,2,1:T(8,128)(2,1)} %all_to_all.20), calls=%async_computation.2 | async-start | bytes 262144 | tf_op jit(solution)/shard_map/all_to_all | solution.py:179
Sparse Core Ops, SparseCore 0:
  11.0 113.5 all-gather.1
  188.7 334.1 reduce-scatter.3
where the time goes:
time: 555 us; the launch traced here: 553 us
  waiting for transfers between devices  388 us (70%)
  local copies, waits for them, and re-layouts  46.7 us (8%)
  other arithmetic  39.2 us (7%)
  matrix products  22.6 us (4%)
  blocking collectives  22.2 us (4%)
  starting transfers between devices  17.9 us (3%)
  between operations  14.4 us (3%)
    unnamed x3, waiting for transfers between devices  333 us
    all_gather x1, waiting for transfers between devices, sent_together(): filled, at, done = (lax.all_gather(both, axis, axis=dim, tiled=True), 0, [])  27 us
    all_to_all x1, blocking collectives, body(): lax.all_to_all(outgoing, 'ep', split_axis=0, concat_axis=0, tiled=True)  22.2 us
    all_to_all x1, waiting for transfers between devices, from_everyone(): lax.all_to_all(jnp.broadcast_to(array[None], (count, *array.shape)), axis...  21.9 us
    another operation x10, other arithmetic  19.9 us
    while x2, local copies, waits for them, and re-layouts, body(): lax.fori_loop(1, seq_devices, visit_gathered, diagonal(query_heads, own_p...  12.8 us
    unnamed x23, local copies, waits for them, and re-layouts  12 us
  transfers between devices with their start and end apart: 4, of which 4 were waited for; matrix products, arithmetic and copies ran while one was open for 7% of the time, Pallas kernels for 0%

commit v1 on v0

v1 whole, which is shorter than its diff:
```python
import functools

import jax
import jax.numpy as jnp
from jax import lax
from jax.experimental import pallas as pl
from jax.experimental.pallas import tpu as pltpu
from jax.sharding import PartitionSpec as P

MESH = pl.DeviceIdType.MESH
BF = jnp.bfloat16
F32 = jnp.float32
NX, NZ, NY = 4, 8, 8
UP, DOWN = 4, 3
LOG2E = 1.4426950408889634
EPS_NORM = 1e-06
ROUTED_SCALE = 2.5
S = 512
H = 128
KVR = 1040
CAPP = 16
CAP = 12


def dot(a, b):
    return jnp.dot(a, b, preferred_element_type=F32)


def iota(shape, dim):
    return lax.broadcasted_iota(jnp.int32, shape, dim)


def attend(query, key, value, bias, diagonal):
    half = S // 2
    logit = lax.dot_general(query, key, (((1,), (1,)), ((), ())), preferred_element_type=F32)
    logit = logit * (LOG2E / H**0.5) + bias
    soft = jnp.maximum(logit, jnp.log2(1.0 + jnp.exp2(jnp.minimum(logit, 100.0))))
    base = logit - soft
    if diagonal:
        visible = iota(soft.shape, 1) < iota(soft.shape, 0)
        soft = jnp.where(visible, soft, 0.0)
    soft = soft.astype(BF)
    later = jnp.where(iota((half, half), 0) > iota((half, half), 1), 1.0, 0.0).astype(BF)
    stay_hi = dot(soft[:, half:], later)
    sum_hi = stay_hi[:, 0:1] + soft[:, half : half + 1].astype(F32)
    stay_lo = dot(soft[:, :half], later) + sum_hi
    total = stay_lo[:, 0:1] + soft[:, 0:1].astype(F32)
    weight = jnp.exp2(base - jnp.concatenate([stay_lo, stay_hi], axis=1))
    if diagonal:
        weight = jnp.where(visible, weight, 0.0)
    return dot(weight.astype(BF), value), total


def kernel(
    q_in, k_in, v_in, bias_in, ow_in, mi_in, gain, ids, scores, sg_in, su_in, sd_in, eg_in, eu_in, ed_in,
    mixed, mix,
    qb, kvb, op, tcol, tr, ts, osend, orecv, oacc, heads,
    wgu, sgu, ed, sd, ow, mi, normed, gated,
    a1s, a1r, a2r, ag, b0, b1r, b2r, common,
    part_m, sib_m, ring_m, rsend_m, part_a, sib_a, ring_a, rsend_a,
    lsem, q_s, q_r, kv_s, kv_r, a1_s, a1_rs, a2_s, a2_rs, ag_s, ag_r, ags_s, ags_r,
    b1_s, b1_rs, b2_s, b2_rs, t_s, t_r, o_s, o_r,
    msib_s, msib_r, mring_s, mring_r, asib_s, asib_r, aring_s, aring_r,
):
    ep, tp = lax.axis_index("ep"), lax.axis_index("tp")
    z, x, y, c = ep // NX, ep % NX, tp // 2, tp % 2

    def at_x(d):
        return {"ep": z * NX + (x + d) % NX, "tp": tp}

    def at_z(d):
        return {"ep": ((z + d) % NZ) * NX + x, "tp": tp}

    def at_y(d):
        return {"ep": ep, "tp": ((y + d) % NY) * 2 + c}

    sibling = {"ep": ep, "tp": y * 2 + (1 - c)}

    def send(src, dst, ssem, rsem, dev):
        return pltpu.make_async_remote_copy(
            src_ref=src, dst_ref=dst, send_sem=ssem, recv_sem=rsem, device_id=dev, device_id_type=MESH
        )

    local = [
        (q_in, qb.at[x]),
        (k_in, kvb.at[z, 0:S]),
        (v_in, kvb.at[z, S : 2 * S]),
        (bias_in, kvb.at[z, 2 * S : KVR]),
        (mi_in, mi),
        (eg_in, wgu.at[:, 0:H]),
        (eu_in, wgu.at[:, H : 2 * H]),
        (sg_in, sgu.at[:, 0:H]),
        (su_in, sgu.at[:, H : 2 * H]),
        (ed_in, ed),
        (sd_in, sd),
        (ow_in, ow),
    ]
    fetch = [pltpu.make_async_copy(a, b, lsem.at[i]) for i, (a, b) in enumerate(local)]
    for f in fetch:
        f.start()

    barrier = pltpu.get_barrier_semaphore()
    partners = [at_x(d) for d in range(1, NX)] + [at_z(d) for d in range(1, NZ)]
    partners += [at_y(1), at_y(-1), sibling]
    for dev in partners:
        pl.semaphore_signal(barrier, inc=1, device_id=dev, device_id_type=MESH)
    pl.semaphore_wait(barrier, len(partners))

    pending = []

    def begin(copy, when=None):
        pending.append((when, copy))
        if when is None:
            copy.start()
        else:
            pl.when(when)(copy.start)

    def up(d):
        block = kvb.at[jnp.maximum(z - d + 1, 0)]
        return send(block, block, kv_s.at[0, d - 1], kv_r.at[0, d - 1], at_z(1))

    def up_arrival(d):
        block = kvb.at[jnp.maximum(z - d, 0)]
        return send(block, block, kv_s.at[0, d - 1], kv_r.at[0, d - 1], at_z(1))

    def down(d):
        block = kvb.at[(z + d - 1) % NZ]
        return send(block, block, kv_s.at[1, d - 1], kv_r.at[1, d - 1], at_z(-1))

    def down_arrival(d):
        block = kvb.at[(z + d) % NZ]
        return send(block, block, kv_s.at[1, d - 1], kv_r.at[1, d - 1], at_z(-1))

    def step(qi, zi, diagonal):
        key, value = kvb[zi, 0:S, :], kvb[zi, S : 2 * S, :]
        rows = kvb[zi, 2 * S : KVR, :].astype(F32) * LOG2E
        bias = jnp.concatenate([rows[j : j + 1, :] for j in range(S // H)], axis=1)
        out, total = attend(qb[qi], key, value, bias, diagonal)
        op[qi, zi] = out
        tcol[qi] = jnp.where(iota((S, H), 1) == zi, total, tcol[qi])

    def attention():
        fetch[0].wait()
        q_out = [send(qb.at[x], qb.at[x], q_s.at[d - 1], q_r.at[d - 1], at_x(d)) for d in range(1, NX)]
        for cp in q_out:
            begin(cp)
        for f in fetch[1:4]:
            f.wait()
        begin(up(1), z < NZ - 1)
        begin(down(1), z < DOWN)
        tcol[...] = jnp.zeros_like(tcol)
        yield
        step(x, z, True)
        yield
        for d in range(1, NX):
            src = qb.at[(x - d + NX) % NX]
            send(src, src, q_s.at[d - 1], q_r.at[d - 1], at_x(d)).wait_recv()

        def own_row(qi, carry):
            @pl.when(qi > x)
            def _():
                step(qi, z, False)

            @pl.when(qi < x)
            def _():
                op[qi, z] = jnp.zeros((S, H), F32)

            return carry

        lax.fori_loop(0, NX, own_row, 0)
        yield

        def all_rows(zi):
            def one(qi, carry):
                step(qi, zi, False)
                return carry

            lax.fori_loop(0, NX, one, 0)

        for d in range(1, UP + 1):

            @pl.when(z >= d)
            def _():
                up_arrival(d).wait_recv()

            if d < UP:
                begin(up(d + 1), (z >= d) & (z < NZ - 1))
            if d <= DOWN:
                came = (z + d) % NZ

                @pl.when(came < DOWN)
                def _():
                    down_arrival(d).wait_recv()

                if d < DOWN:
                    begin(down(d + 1), came < DOWN)

            @pl.when(z >= d)
            def _():
                all_rows(jnp.maximum(z - d, 0))

            yield
            if d <= DOWN:

                @pl.when((came < DOWN) & (came < z))
                def _():
                    all_rows(came)

                yield
        for qi in range(NX):
            ts[qi] = tcol[qi].T[0:NZ, :]
        for d in range(1, NX):
            begin(send(ts, tr.at[x], t_s.at[d - 1], t_r.at[d - 1], at_x(d)))
        tr[x] = ts[...]
        yield
        for d in range(1, NX):
            src = tr.at[(x - d + NX) % NX]
            send(ts, src, t_s.at[d - 1], t_r.at[d - 1], at_x(d)).wait_recv()

        def combine(qi):
            sums = [tr[i, qi] for i in range(NX)]
            row = sums[0] + sums[1] + sums[2] + sums[3]
            within = sum(jnp.where(i > x, sums[i], 0.0) for i in range(1, NX))
            parts, run = [], jnp.zeros((1, S), F32)
            for zi in reversed(range(NZ)):
                parts.append(run)
                run = run + row[zi : zi + 1, :]
            carried = jnp.concatenate(parts[::-1], axis=0) + within
            scale = jnp.exp2(-carried)
            scale = jnp.concatenate([scale, jnp.zeros((H - NZ, S), F32)], axis=0).T
            for zi in range(NZ):
                if zi == 0:
                    oacc[...] = scale[:, 0:1] * op[qi, 0]
                else:

                    @pl.when(zi <= z)
                    def _():
                        oacc[...] += scale[:, zi : zi + 1] * op[qi, zi]

        for d in range(1, NX):
            qi = (x + d) % NX
            combine(qi)
            osend[d - 1] = oacc[...].astype(BF)
            begin(send(osend.at[d - 1], orecv.at[d - 1], o_s.at[d - 1], o_r.at[d - 1], at_x(d)))
        combine(x)
        yield
        for d in range(1, NX):
            send(osend.at[d - 1], orecv.at[d - 1], o_s.at[d - 1], o_r.at[d - 1], at_x(d)).wait_recv()
        total = oacc[...]
        for d in range(1, NX):
            total = total + orecv[d - 1].astype(F32)
        heads[...] = total.astype(BF)
        fetch[11].wait()
        for yi in range(NY):
            both = dot(heads[...], ow[:, yi * 256 : (yi + 1) * 256]).astype(BF)
            part_a[0, yi] = both[:, :H]
            part_a[1, yi] = both[:, H:]
        out = yield from reduce_scatter(part_a, sib_a, ring_a, rsend_a, asib_s, asib_r, aring_s, aring_r)
        mixed[...] = out.astype(BF)

    def reduce_scatter(part, sib, ring, rsend, sib_s, sib_r, ring_s, ring_r):
        order = [4, -3, 3, -2, 2, -1, 1, 0]

        def to_sibling(m):
            yi = (y + order[m] + NY) % NY
            return send(part.at[1 - c, yi], sib.at[m], sib_s.at[m], sib_r.at[m], sibling)

        for m in range(NY):
            begin(to_sibling(m))
        yield

        def mine(m):
            to_sibling(m).wait_recv()
            yi = (y + order[m] + NY) % NY
            return part[c, yi].astype(F32) + sib[m].astype(F32)

        def hop(way, s):
            return send(
                rsend.at[way, s], ring.at[way, s], ring_s.at[way, s], ring_r.at[way, s], at_y(1 - 2 * way)
            )

        for s in range(4):
            for way in range(2):
                if way == 1 and s == 3:
                    continue
                value = mine(2 * s + way)
                if s > 0:
                    hop(way, s - 1).wait_recv()
                    value = value + ring[way, s - 1].astype(F32)
                rsend[way, s] = value.astype(BF)
                begin(hop(way, s))
            yield
        value = mine(7)
        hop(1, 2).wait_recv()
        value = value + ring[1, 2].astype(F32)
        hop(0, 3).wait_recv()
        return value + ring[0, 3].astype(F32)

    def spread(transposed):
        shape = (NZ * NX * CAPP, NZ * NX * CAP) if transposed else (NZ * NX * CAP, NZ * NX * CAPP)
        padded, packed = (iota(shape, 0), iota(shape, 1)) if transposed else (iota(shape, 1), iota(shape, 0))
        place = padded & (CAPP - 1)
        hit = ((padded >> 4) * CAP + place == packed) & (place < CAP)
        return jnp.where(hit, 1.0, 0.0).astype(BF)

    def experts():
        fetch[4].wait()
        value = mi[...].astype(F32)
        mean = jnp.mean(value * value, axis=1, keepdims=True)
        normed[...] = (value * lax.rsqrt(mean + EPS_NORM) * gain[...]).astype(BF)
        own = normed[:, pl.ds(pl.multiple_of(tp * H, H), H)]
        slots = NZ * NX * CAPP
        group = iota((slots, 128), 0) >> 4
        place = iota((slots, 128), 0) & (CAPP - 1)
        expert = (group & (NZ - 1)) * NX + (group >> 3)
        first, second = ids[0:1, :] == expert, ids[1:2, :] == expert
        named = first | second
        earlier = jnp.where(iota((128, 128), 0) < iota((128, 128), 1), 1.0, 0.0).astype(BF)
        count = dot(jnp.where(named, 1.0, 0.0).astype(BF), earlier)
        chosen = named & (count == place.astype(F32))
        scale = ROUTED_SCALE / (scores[0:1, :] + scores[1:2, :])
        gate = jnp.where(first, scores[0:1, :] * scale, 0.0) + jnp.where(second, scores[1:2, :] * scale, 0.0)
        gated[...] = jnp.where(chosen, gate, 0.0)
        out = dot(jnp.where(chosen, 1.0, 0.0).astype(BF), own).astype(BF)
        a1s[...] = out.reshape(NX, NZ, CAPP, H)

        def by_x(d):
            return send(a1s.at[(x + d) % NX], a1r.at[x], a1_s.at[d - 1], a1_rs.at[d - 1], at_x(d))

        for d in range(1, NX):
            begin(by_x(d))
        a1r[x] = a1s[x]
        yield
        for d in range(1, NX):
            send(a1s.at[x], a1r.at[(x - d + NX) % NX], a1_s.at[d - 1], a1_rs.at[d - 1], at_x(d)).wait_recv()
        for d in range(1, NZ):
            begin(send(a1r.at[:, (z + d) % NZ], a2r.at[z], a2_s.at[d - 1], a2_rs.at[d - 1], at_z(d)))
        a2r[z] = a1r[:, z]
        yield
        for d in range(1, NZ):
            send(a1r.at[:, z], a2r.at[(z - d + NZ) % NZ], a2_s.at[d - 1], a2_rs.at[d - 1], at_z(d)).wait_recv()
        packed = dot(spread(False), a2r[...].reshape(slots, H)).astype(BF)
        ag[tp] = packed

        def along(way, s):
            sign = 1 - 2 * way
            mine = ag.at[((y - sign * (s - 1) + NY) % NY) * 2 + c]
            return send(mine, mine, ag_s.at[way, s - 1], ag_r.at[way, s - 1], at_y(sign))

        def arrival(way, s):
            sign = 1 - 2 * way
            theirs = ag.at[((y - sign * s + NY) % NY) * 2 + c]
            return send(theirs, theirs, ag_s.at[way, s - 1], ag_r.at[way, s - 1], at_y(sign))

        def across(m, yi, core):
            ref = ag.at[yi * 2 + core]
            return send(ref, ref, ags_s.at[m], ags_r.at[m], sibling)

        begin(along(0, 1))
        begin(along(1, 1))
        begin(across(0, y, c))
        yield
        for s in range(1, 5):
            for way in range(2):
                if way == 1 and s == 4:
                    continue
                arrival(way, s).wait_recv()
                if s < 4 - way:
                    begin(along(way, s + 1))
                sign = 1 - 2 * way
                begin(across(way * 4 + s, (y - sign * s + NY) % NY, c))
            yield
        across(0, y, 1 - c).wait_recv()
        for s in range(1, 5):
            for way in range(2):
                if way == 1 and s == 4:
                    continue
                sign = 1 - 2 * way
                across(way * 4 + s, (y - sign * s + NY) % NY, 1 - c).wait_recv()
        for i in (5, 6, 7, 8, 9, 10):
            fetch[i].wait()
        acc = jnp.zeros((NZ * NX * CAP, 2 * H), F32)
        acc_s = jnp.zeros((128, 2 * H), F32)
        for j in range(NY):
            wide = jnp.concatenate([ag[2 * j], ag[2 * j + 1]], axis=1)
            acc = acc + dot(wide, wgu[j * 256 : (j + 1) * 256, :])
            acc_s = acc_s + dot(normed[:, j * 256 : (j + 1) * 256], sgu[j * 256 : (j + 1) * 256, :])

        def swiglu(a):
            g, u = a[:, :H], a[:, H:]
            return (g / (1.0 + jnp.exp(-g)) * u).astype(BF)

        hidden, hidden_s = swiglu(acc), swiglu(acc_s)
        rows = NZ * NX * CAP
        for yi in range(NY):
            cols = slice(yi * 256, (yi + 1) * 256)
            both = dot(hidden, ed[:, cols]).astype(BF)
            part_m[0, yi, 0:rows] = both[:, :H]
            part_m[1, yi, 0:rows] = both[:, H:]
            both = dot(hidden_s, sd[:, cols]).astype(BF)
            part_m[0, yi, rows:S] = both[:, :H]
            part_m[1, yi, rows:S] = both[:, H:]
        out = yield from reduce_scatter(part_m, sib_m, ring_m, rsend_m, msib_s, msib_r, mring_s, mring_r)
        common[...] = out[rows:S, :]
        b0[...] = dot(spread(True), out[0:rows, :].astype(BF)).astype(BF).reshape(NZ, NX, CAPP, H)
        for d in range(1, NZ):
            begin(send(b0.at[(z + d) % NZ], b1r.at[z], b1_s.at[d - 1], b1_rs.at[d - 1], at_z(d)))
        b1r[z] = b0[z]
        yield
        for d in range(1, NZ):
            send(b0.at[z], b1r.at[(z - d + NZ) % NZ], b1_s.at[d - 1], b1_rs.at[d - 1], at_z(d)).wait_recv()
        for d in range(1, NX):
            begin(send(b1r.at[:, (x + d) % NX], b2r.at[x], b2_s.at[d - 1], b2_rs.at[d - 1], at_x(d)))
        b2r[x] = b1r[:, x]
        yield
        for d in range(1, NX):
            send(b1r.at[:, x], b2r.at[(x - d + NX) % NX], b2_s.at[d - 1], b2_rs.at[d - 1], at_x(d)).wait_recv()
        gates = gated[...].T
        high = gates.astype(BF)
        low = (gates - high.astype(F32)).astype(BF)
        got = b2r[...].reshape(slots, H)
        mix[...] = (common[...] + dot(high, got) + dot(low, got)).astype(BF)

    def advance(work):
        try:
            next(work)
            return True
        except StopIteration:
            return False

    attn, moe = attention(), experts()
    live = [True, True]
    while any(live):
        live[0] = live[0] and advance(attn)
        live[1] = live[1] and advance(moe)

    for when, copy in pending:
        if when is None:
            copy.wait_send()
        else:
            pl.when(when)(copy.wait_send)


def body(
    queries, keys, values, key_bias, out_weight, moe_input, moe_gain, route_ids, route_scores,
    shared_gate, shared_up, shared_down, expert_gate, expert_up, expert_down,
):
    bias = jnp.pad(key_bias.reshape(S // H, H), ((0, KVR - 2 * S - S // H), (0, 0)))
    ids = jnp.pad(route_ids.T, ((0, 6), (0, 0)))
    scores = jnp.pad(route_scores.T, ((0, 6), (0, 0)))
    hbm, vmem = pl.BlockSpec(memory_space=pl.ANY), pl.BlockSpec(memory_space=pltpu.VMEM)
    dma = pltpu.SemaphoreType.DMA
    V = pltpu.VMEM
    slots = (NZ, NX, CAPP, H)
    rs = [V((2, NY, S, H), BF), V((NY, S, H), BF), V((2, 4, S, H), BF), V((2, 4, S, H), BF)]
    sems = [dma((12,)), dma((3,)), dma((3,)), dma((2, 4)), dma((2, 4)), dma((3,)), dma((3,)), dma((7,)), dma((7,))]
    sems += [dma((2, 4)), dma((2, 4)), dma((8,)), dma((8,))]
    sems += [dma((7,)), dma((7,)), dma((3,)), dma((3,)), dma((3,)), dma((3,)), dma((3,)), dma((3,))]
    sems += [dma((8,)), dma((8,)), dma((2, 4)), dma((2, 4))] * 2
    return pl.pallas_call(
        kernel,
        out_shape=(jax.ShapeDtypeStruct((S, H), BF), jax.ShapeDtypeStruct((128, H), BF)),
        in_specs=[hbm] * 6 + [vmem] * 3 + [hbm] * 6,
        out_specs=(vmem, vmem),
        scratch_shapes=[
            V((NX, S, H), BF), V((NZ, KVR, H), BF), V((NX, NZ, S, H), F32), V((NX, S, H), F32),
            V((NX, NX, NZ, S), F32), V((NX, NZ, S), F32), V((NX - 1, S, H), BF), V((NX - 1, S, H), BF),
            V((S, H), F32), V((S, H), BF),
            V((2048, 2 * H), BF), V((2048, 2 * H), BF), V((H, 2048), BF), V((H, 2048), BF), V((H, 2048), BF),
            V((128, 2048), BF), V((128, 2048), BF), V((512, 128), F32),
            V((NX, NZ, CAPP, H), BF), V((NX, NZ, CAPP, H), BF), V(slots, BF), V((16, NZ * NX * CAP, H), BF),
            V(slots, BF), V(slots, BF), V((NX, NZ, CAPP, H), BF), V((128, H), F32),
            *rs, *rs, *sems,
        ],
        compiler_params=pltpu.CompilerParams(
            collective_id=0, has_side_effects=True, vmem_limit_bytes=60 * 2**20
        ),
        name="fused",
    )(
        queries, keys, values, bias, out_weight, moe_input, moe_gain.reshape(1, -1), ids, scores,
        shared_gate, shared_up, shared_down,
        expert_gate.reshape(2048, H), expert_up.reshape(2048, H), expert_down.reshape(H, 2048),
    )


def solution(mesh):
    return jax.shard_map(
        body,
        mesh=mesh,
        in_specs=(
            P("ep", "tp"), P("ep", "tp"), P("ep", "tp"), P("ep", "tp"), P("tp", None), P("ep", None), P(),
            P("ep", None), P("ep", None), P(None, "tp"), P(None, "tp"), P("tp", None),
            P("ep", None, "tp"), P("ep", None, "tp"), P("ep", "tp", None),
        ),
        out_specs=(P("ep", "tp"), P("ep", "tp")),
        check_vma=False,
    )
```

time: 555 us -> 102 us (0.18)
  waiting for transfers between devices: 388 us -> 0 us
  Pallas kernels: 0 us -> 95.1 us
  local copies, waits for them, and re-layouts: 46.7 us -> 4.81 us
  other arithmetic: 39.2 us -> 0.02 us
  matrix products: 22.6 us -> 0 us
  blocking collectives: 22.2 us -> 0 us
  starting transfers between devices: 17.9 us -> 0 us
  between operations: 14.4 us -> 0.67 us
    unnamed x3 -> x0, waiting for transfers between devices: 333 us -> none
    pallas_call x0 -> x1, Pallas kernels: none -> 95.1 us  [body(): pl.pallas_call(kernel, out_shape=(jax.ShapeDtypeStruct((S, H), BF), jax.S...]
    all_to_all x2 -> x0, waiting for transfers between devices: 28 us -> none  [the longest x1 21.9 us: from_everyone(): lax.all_to_all(jnp.broadcast_to(array[None], (count, *array.shape)), axis...]
    all_gather x1 -> x0, waiting for transfers between devices: 27 us -> none  [sent_together(): filled, at, done = (lax.all_gather(both, axis, axis=dim, tiled=True), 0, [])]
    dot_general x15 -> x0, matrix products: 22.6 us -> none  [the longest x4 8.01 us: absorb(): jnp.einsum('qhd,khd->hqk', query_heads, key_heads, preferred_element_type...]
    all_to_all x1 -> x0, blocking collectives: 22.2 us -> none  [body(): lax.all_to_all(outgoing, 'ep', split_axis=0, concat_axis=0, tiled=True)]
    another operation x10 -> x0, other arithmetic: 19.9 us -> none
    all_to_all x2 -> x0, starting transfers between devices: 17.8 us -> none  [the longest x1 10.7 us: body(): lax.all_to_all(routed_sum, 'ep', split_axis=1, concat_axis=1, tiled=True)]
  transfers between devices with their start and end apart: 4 -> 0, of which waited for: 4 -> 0; matrix products, arithmetic and copies ran while one was open for 7% -> 0% of each run, Pallas kernels for 0% -> 0%
where the time goes in v1:
time: 102 us; the launch traced here: 101 us
  Pallas kernels  95.1 us (93%)
  local copies, waits for them, and re-layouts  4.81 us (5%)
    pallas_call x1, Pallas kernels, body(): pl.pallas_call(kernel, out_shape=(jax.ShapeDtypeStruct((S, H), BF), jax.S...  95.1 us
    unnamed x10, local copies, waits for them, and re-layouts  3.03 us

profile of v1, /device:TPU:6, one launch (start us, length us, event | category | flops | bytes accessed | tf_op | source)
XLA Modules:
  0.0 100.6 jit_solution(15459076273491549122)
XLA Ops:
  0.6 0.0 copy-start.1
  0.6 0.7 copy-done.1
  1.3 0.0 copy-start.2
  1.3 0.6 pad.12.bias_in
  1.9 0.1 copy-done.2
  2.0 0.0 copy-start.3
  2.0 0.6 pad.13.ids
  2.6 0.1 copy-done.3
  2.7 0.6 pad.14.scores
  3.3 95.1 %fused.1 = (bf16[512,128]{1,0:T(8,128)(2,1)}, bf16[128,128]{1,0:T(8,128)(2,1)}) custom-call(bf16[512,128]{1,0:T(8,128)(2,1)} %q_in.1, bf16[512,128]{1,0:T(8,128)(2,1)} %k_in.1, bf16[512,128]{1,0:T(8,128)(2,1)} %v_in.1, bf16[16,128]{1,0:T(8,128)(2,1)} %pad.12.bias_in, bf16[128,2048]{1,0:T(8,128)(2,1)} %ow_in.1, bf16[128,2048]{1,0:T(8,128)(2,1)} %mi_in.1, ...), custom_call_target="tpu_custom_call" | custom-call | tf_op jit(solution)/shard_map/fused/pallas_call | solution.py:460
  98.4 0.0 copy-start
  98.4 1.6 %copy.19 = bf16[512,128]{1,0:T(8,128)(2,1)} copy(bf16[512,128]{1,0:T(8,128)(2,1)} %get-tuple-element.4) | data formatting | bytes 262144
  99.9 0.0 copy-done
  99.9 0.6 copy.20
  (1 shorter events, 0.0 us)
Async XLA Ops:
  0.6 0.7 copy-start.1
  1.3 0.7 copy-start.2
  2.0 0.7 copy-start.3
  98.4 1.6 %copy-start = (bf16[128,128]{1,0:T(8,128)(2,1)S(1)}, bf16[128,128]{1,0:T(8,128)(2,1)}, u32[]{:S(2)}) copy-start(bf16[128,128]{1,0:T(8,128)(2,1)} %get-tuple-element.5) | copy-start | bytes 98308

commit v2 on v1

v2 whole, which is shorter than its diff:
```python
import functools

import jax
import jax.numpy as jnp
from jax import lax
from jax.experimental import pallas as pl
from jax.experimental.pallas import tpu as pltpu
from jax.sharding import PartitionSpec as P

MESH = pl.DeviceIdType.MESH
BF = jnp.bfloat16
F32 = jnp.float32
NX, NZ, NY = 4, 8, 8
UP, DOWN = 4, 3
LOG2E = 1.4426950408889634
EPS_NORM = 1e-06
ROUTED_SCALE = 2.5
S = 512
H = 128
KB = 528
KVR = 1040
CAPP = 16
CAP = 12


def dot(a, b):
    return jnp.dot(a, b, preferred_element_type=F32)


def iota(shape, dim):
    return lax.broadcasted_iota(jnp.int32, shape, dim)


def attend(query, key, value, bias, first):
    half = S // 2
    logit = lax.dot_general(query, key, (((1,), (1,)), ((), ())), preferred_element_type=F32)
    logit = logit * (LOG2E / H**0.5) + bias
    soft = jnp.maximum(logit, jnp.log2(1.0 + jnp.exp2(jnp.minimum(logit, 100.0))))
    base = logit - soft
    if first is not None:
        visible = iota(soft.shape, 1) + first < iota(soft.shape, 0)
        soft = jnp.where(visible, soft, 0.0)
    soft = soft.astype(BF)
    later = jnp.where(iota((half, half), 0) > iota((half, half), 1), 1.0, 0.0).astype(BF)
    stay_hi = dot(soft[:, half:], later)
    sum_hi = stay_hi[:, 0:1] + soft[:, half : half + 1].astype(F32)
    stay_lo = dot(soft[:, :half], later) + sum_hi
    total = stay_lo[:, 0:1] + soft[:, 0:1].astype(F32)
    weight = jnp.exp2(base - jnp.concatenate([stay_lo, stay_hi], axis=1))
    if first is not None:
        weight = jnp.where(visible, weight, 0.0)
    return dot(weight.astype(BF), value), total


def kernel(
    q_in, k_in, v_in, bias_in, ow_in, mi_in, gain_in, ids_in, scores_in, sg_in, su_in, sd_in, eg_in, eu_in, ed_in,
    mixed, mix,
    qb, kvb, op, tcol, tr, ts, osend, orecv, oacc, heads,
    bias, gain, ids, scores, wgu, sgu, ed, sd, ow, mi, normed, gated,
    a1s, a1r, a2r, ag, b0, b1r, b2r, common,
    part_m, sib_m, ring_m, rsend_m, part_a, sib_a, ring_a, rsend_a,
    lsem, q_s, q_r, kv_s, kv_r, a1_s, a1_rs, a2_s, a2_rs, ag_s, ag_r, ags_s, ags_r,
    b1_s, b1_rs, b2_s, b2_rs, t_s, t_r, o_s, o_r,
    msib_s, msib_r, mring_s, mring_r, asib_s, asib_r, aring_s, aring_r,
):
    ep, tp = lax.axis_index("ep"), lax.axis_index("tp")
    z, x, y, c = ep // NX, ep % NX, tp // 2, tp % 2

    def at_x(d):
        return {"ep": z * NX + (x + d) % NX, "tp": tp}

    def at_z(d):
        return {"ep": ((z + d) % NZ) * NX + x, "tp": tp}

    def at_y(d):
        return {"ep": ep, "tp": ((y + d) % NY) * 2 + c}

    sibling = {"ep": ep, "tp": y * 2 + (1 - c)}

    def send(src, dst, ssem, rsem, dev):
        return pltpu.make_async_remote_copy(
            src_ref=src, dst_ref=dst, send_sem=ssem, recv_sem=rsem, device_id=dev, device_id_type=MESH
        )

    local = [
        (q_in, qb.at[pl.ds(pl.multiple_of(x * S, S), S)]),
        (k_in, kvb.at[z, 0:S]),
        (v_in, kvb.at[z, KB:KVR]),
        (bias_in, bias),
        (mi_in, mi),
        (eg_in, wgu.at[:, 0:H]),
        (eu_in, wgu.at[:, H : 2 * H]),
        (sg_in, sgu.at[:, 0:H]),
        (su_in, sgu.at[:, H : 2 * H]),
        (ed_in, ed),
        (sd_in, sd),
        (ow_in, ow),
        (gain_in, gain),
        (ids_in, ids),
        (scores_in, scores),
    ]
    fetch = [pltpu.make_async_copy(a, b, lsem.at[i]) for i, (a, b) in enumerate(local)]

    barrier = pltpu.get_barrier_semaphore()
    partners = [at_x(d) for d in range(1, NX)] + [at_z(d) for d in range(1, NZ)]
    partners += [at_y(1), at_y(-1), sibling]
    for dev in partners:
        pl.semaphore_signal(barrier, inc=1, device_id=dev, device_id_type=MESH)
    for i in (4, 12, 13, 14, 3, 0, 1, 2, 5, 6, 7, 8, 9, 10, 11):
        fetch[i].start()

    pending = []

    def begin(copy, when=None):
        pending.append((when, copy))
        if when is None:
            copy.start()
        else:
            pl.when(when)(copy.start)

    halves = (slice(0, KB), slice(KB, KVR))

    def query_rows(i):
        return qb.at[pl.ds(pl.multiple_of(i * S, S), S)]

    def up(d, h):
        block = kvb.at[jnp.maximum(z - d + 1, 0), halves[h]]
        return send(block, block, kv_s.at[0, d - 1, h], kv_r.at[0, d - 1, h], at_z(1))

    def up_arrival(d, h):
        block = kvb.at[jnp.maximum(z - d, 0), halves[h]]
        return send(block, block, kv_s.at[0, d - 1, h], kv_r.at[0, d - 1, h], at_z(1))

    def down(d, h):
        block = kvb.at[(z + d - 1) % NZ, halves[h]]
        return send(block, block, kv_s.at[1, d - 1, h], kv_r.at[1, d - 1, h], at_z(-1))

    def down_arrival(d, h):
        block = kvb.at[(z + d) % NZ, halves[h]]
        return send(block, block, kv_s.at[1, d - 1, h], kv_r.at[1, d - 1, h], at_z(-1))

    def step(zi, first):
        rows = kvb[zi, S:KB, :].astype(F32) * LOG2E
        row = jnp.concatenate([rows[j : j + 1, :] for j in range(S // H)], axis=1)
        out, total = attend(qb[...], kvb[zi, 0:S, :], kvb[zi, KB:KVR, :], row, first)
        op[zi] = out
        tcol[...] = jnp.where(iota((NX * S, H), 1) == zi, total, tcol[...])

    def attention():
        fetch[0].wait()
        for d in range(1, NX):
            begin(send(query_rows(x), query_rows(x), q_s.at[d - 1], q_r.at[d - 1], at_x(d)))
        fetch[1].wait()
        begin(up(1, 0), z < NZ - 1)
        begin(down(1, 0), z < DOWN)
        yield
        fetch[2].wait()
        begin(up(1, 1), z < NZ - 1)
        begin(down(1, 1), z < DOWN)
        tcol[...] = jnp.zeros_like(tcol)
        for d in range(1, NX):
            src = query_rows((x - d + NX) % NX)
            send(src, src, q_s.at[d - 1], q_r.at[d - 1], at_x(d)).wait_recv()
        step(z, x * S)
        yield
        for d in range(1, UP + 1):
            came = (z + d) % NZ
            for h in range(2):

                @pl.when(z >= d)
                def _():
                    up_arrival(d, h).wait_recv()

                if d < UP:
                    begin(up(d + 1, h), (z >= d) & (z < NZ - 1))
                if d <= DOWN:

                    @pl.when(came < DOWN)
                    def _():
                        down_arrival(d, h).wait_recv()

                    if d < DOWN:
                        begin(down(d + 1, h), came < DOWN)

            @pl.when(z >= d)
            def _():
                step(jnp.maximum(z - d, 0), None)

            yield
            if d <= DOWN:

                @pl.when((came < DOWN) & (came < z))
                def _():
                    step(came, None)

                yield
        for qi in range(NX):
            ts[qi] = tcol[qi * S : (qi + 1) * S].T[0:NZ, :]
        for d in range(1, NX):
            begin(send(ts, tr.at[x], t_s.at[d - 1], t_r.at[d - 1], at_x(d)))
        tr[x] = ts[...]
        yield
        for d in range(1, NX):
            src = tr.at[(x - d + NX) % NX]
            send(ts, src, t_s.at[d - 1], t_r.at[d - 1], at_x(d)).wait_recv()

        def combine(qi):
            sums = [tr[i, qi] for i in range(NX)]
            row = sums[0] + sums[1] + sums[2] + sums[3]
            within = sum(jnp.where(i > x, sums[i], 0.0) for i in range(1, NX))
            parts, run = [], jnp.zeros((1, S), F32)
            for zi in reversed(range(NZ)):
                parts.append(run)
                run = run + row[zi : zi + 1, :]
            carried = jnp.concatenate(parts[::-1], axis=0) + within
            scale = jnp.exp2(-carried)
            scale = jnp.concatenate([scale, jnp.zeros((H - NZ, S), F32)], axis=0).T
            rows = pl.ds(pl.multiple_of(qi * S, S), S)
            oacc[...] = scale[:, 0:1] * op[0, rows, :]
            for zi in range(1, NZ):

                @pl.when(zi <= z)
                def _():
                    oacc[...] += scale[:, zi : zi + 1] * op[zi, rows, :]

        for d in range(1, NX):
            qi = (x + d) % NX
            combine(qi)
            osend[d - 1] = oacc[...].astype(BF)
            begin(send(osend.at[d - 1], orecv.at[d - 1], o_s.at[d - 1], o_r.at[d - 1], at_x(d)))
        combine(x)
        yield
        for d in range(1, NX):
            send(osend.at[d - 1], orecv.at[d - 1], o_s.at[d - 1], o_r.at[d - 1], at_x(d)).wait_recv()
        total = oacc[...]
        for d in range(1, NX):
            total = total + orecv[d - 1].astype(F32)
        heads[...] = total.astype(BF)
        fetch[11].wait()

        def fill(yi):
            both = dot(heads[...], ow[:, pl.ds(pl.multiple_of(yi * 256, 256), 256)]).astype(BF)
            part_a[0, yi] = both[:, :H]
            part_a[1, yi] = both[:, H:]

        out = yield from reduce_scatter(
            fill, 2, part_a, sib_a, ring_a, rsend_a, asib_s, asib_r, aring_s, aring_r
        )
        mixed[...] = out.astype(BF)

    def reduce_scatter(fill, cuts, part, sib, ring, rsend, sib_s, sib_r, ring_s, ring_r):
        order = [4, -3, 3, -2, 2, -1, 1, 0]
        length = S // cuts
        spans = [slice(i * length, (i + 1) * length) for i in range(cuts)]

        def to_sibling(m):
            yi = (y + order[m] + NY) % NY
            return send(part.at[1 - c, yi], sib.at[m], sib_s.at[m], sib_r.at[m], sibling)

        for m in range(NY):
            fill((y + order[m] + NY) % NY)
            begin(to_sibling(m))
        yield

        def mine(m, span):
            yi = (y + order[m] + NY) % NY
            return part[c, yi, span].astype(F32) + sib[m, span].astype(F32)

        def hop(way, s, i):
            return send(
                rsend.at[way, s, spans[i]], ring.at[way, s, spans[i]],
                ring_s.at[way, s, i], ring_r.at[way, s, i], at_y(1 - 2 * way),
            )

        for s in range(4):
            for i in range(cuts):
                for way in range(2):
                    if way == 1 and s == 3:
                        continue
                    if i == 0:
                        to_sibling(2 * s + way).wait_recv()
                    value = mine(2 * s + way, spans[i])
                    if s > 0:
                        hop(way, s - 1, i).wait_recv()
                        value = value + ring[way, s - 1, spans[i]].astype(F32)
                    rsend[way, s, spans[i]] = value.astype(BF)
                    begin(hop(way, s, i))
            yield
        to_sibling(7).wait_recv()
        done = []
        for i in range(cuts):
            value = mine(7, spans[i])
            hop(1, 2, i).wait_recv()
            value = value + ring[1, 2, spans[i]].astype(F32)
            hop(0, 3, i).wait_recv()
            done.append(value + ring[0, 3, spans[i]].astype(F32))
        return jnp.concatenate(done, axis=0) if cuts > 1 else done[0]

    def spread(transposed):
        shape = (NZ * NX * CAPP, NZ * NX * CAP) if transposed else (NZ * NX * CAP, NZ * NX * CAPP)
        padded, packed = (iota(shape, 0), iota(shape, 1)) if transposed else (iota(shape, 1), iota(shape, 0))
        place = padded & (CAPP - 1)
        hit = ((padded >> 4) * CAP + place == packed) & (place < CAP)
        return jnp.where(hit, 1.0, 0.0).astype(BF)

    def experts():
        for i in (4, 12, 13, 14):
            fetch[i].wait()
        value = mi[...].astype(F32)
        mean = jnp.mean(value * value, axis=1, keepdims=True)
        normed[...] = (value * lax.rsqrt(mean + EPS_NORM) * gain[...]).astype(BF)
        facing = ((y + NY // 2) % NY) * 2 + c
        own = jnp.concatenate([normed[:, pl.ds(pl.multiple_of(i * H, H), H)] for i in (tp, facing)], axis=1)
        slots = NZ * NX * CAPP
        group = iota((slots, 128), 0) >> 4
        place = iota((slots, 128), 0) & (CAPP - 1)
        expert = (group & (NZ - 1)) * NX + (group >> 3)
        first, second = ids[0:1, :] == expert, ids[1:2, :] == expert
        named = first | second
        earlier = jnp.where(iota((128, 128), 0) < iota((128, 128), 1), 1.0, 0.0).astype(BF)
        count = dot(jnp.where(named, 1.0, 0.0).astype(BF), earlier)
        chosen = named & (count == place.astype(F32))
        scale = ROUTED_SCALE / (scores[0:1, :] + scores[1:2, :])
        gate = jnp.where(first, scores[0:1, :] * scale, 0.0) + jnp.where(second, scores[1:2, :] * scale, 0.0)
        gated[...] = jnp.where(chosen, gate, 0.0)
        out = dot(jnp.where(chosen, 1.0, 0.0).astype(BF), own).astype(BF)
        a1s[...] = out.reshape(NX, NZ, CAPP, 2 * H)
        fetch[3].wait()
        line = bias[...]
        line = [line[:, j * H : (j + 1) * H] for j in range(S // H)]
        kvb[z, S:KB, :] = jnp.concatenate(line + [jnp.zeros((KB - S - S // H, H), BF)], axis=0)
        pl.semaphore_wait(barrier, len(partners))

        def by_x(d):
            return send(a1s.at[(x + d) % NX], a1r.at[x], a1_s.at[d - 1], a1_rs.at[d - 1], at_x(d))

        for d in range(1, NX):
            begin(by_x(d))
        a1r[x] = a1s[x]
        yield
        for d in range(1, NX):
            send(a1s.at[x], a1r.at[(x - d + NX) % NX], a1_s.at[d - 1], a1_rs.at[d - 1], at_x(d)).wait_recv()
        for d in range(1, NZ):
            begin(send(a1r.at[:, (z + d) % NZ], a2r.at[z], a2_s.at[d - 1], a2_rs.at[d - 1], at_z(d)))
        a2r[z] = a1r[:, z]
        yield
        for d in range(1, NZ):
            send(a1r.at[:, z], a2r.at[(z - d + NZ) % NZ], a2_s.at[d - 1], a2_rs.at[d - 1], at_z(d)).wait_recv()
        packed = dot(spread(False), a2r[...].reshape(slots, 2 * H)).astype(BF)
        ag[tp] = packed[:, :H]
        ag[facing] = packed[:, H:]

        def slice_of(yi, core=c):
            return ag.at[((yi + NY) % NY) * 2 + core]

        def along(way, n, yi):
            return send(slice_of(yi), slice_of(yi), ag_s.at[way, n], ag_r.at[way, n], at_y(1 - 2 * way))

        def across(m, yi, core):
            return send(slice_of(yi, core), slice_of(yi, core), ags_s.at[m], ags_r.at[m], sibling)

        for n in range(2):
            for way in range(2):
                begin(along(way, n, y + n * NY // 2))
        begin(across(0, y, c))
        begin(across(1, y + NY // 2, c))
        yield
        for way in range(2):
            near = y - (1 - 2 * way)
            along(way, 0, near).wait_recv()
            begin(along(way, 2, near))
            begin(across(2 + way, near, c))
        yield
        for n in range(1, 3):
            for way in range(2):
                sign = 1 - 2 * way
                came = y - sign + NY // 2 if n == 1 else y - 2 * sign
                along(way, n, came).wait_recv()
                begin(across(2 + 2 * n + way, came, c))
        yield
        across(0, y, 1 - c).wait_recv()
        across(1, y + NY // 2, 1 - c).wait_recv()
        for way in range(2):
            sign = 1 - 2 * way
            across(2 + way, y - sign, 1 - c).wait_recv()
            across(4 + way, y - sign + NY // 2, 1 - c).wait_recv()
            across(6 + way, y - 2 * sign, 1 - c).wait_recv()
        for i in (5, 6, 7, 8, 9, 10):
            fetch[i].wait()
        acc = jnp.zeros((NZ * NX * CAP, 2 * H), F32)
        acc_s = jnp.zeros((128, 2 * H), F32)
        for j in range(NY):
            wide = jnp.concatenate([ag[2 * j], ag[2 * j + 1]], axis=1)
            acc = acc + dot(wide, wgu[j * 256 : (j + 1) * 256, :])
            acc_s = acc_s + dot(normed[:, j * 256 : (j + 1) * 256], sgu[j * 256 : (j + 1) * 256, :])

        def swiglu(a):
            g, u = a[:, :H], a[:, H:]
            return (g / (1.0 + jnp.exp(-g)) * u).astype(BF)

        hidden, hidden_s = swiglu(acc), swiglu(acc_s)
        rows = NZ * NX * CAP

        def fill(yi):
            cols = pl.ds(pl.multiple_of(yi * 256, 256), 256)
            both = dot(hidden, ed[:, cols]).astype(BF)
            part_m[0, yi, 0:rows] = both[:, :H]
            part_m[1, yi, 0:rows] = both[:, H:]
            both = dot(hidden_s, sd[:, cols]).astype(BF)
            part_m[0, yi, rows:S] = both[:, :H]
            part_m[1, yi, rows:S] = both[:, H:]

        out = yield from reduce_scatter(
            fill, 1, part_m, sib_m, ring_m, rsend_m, msib_s, msib_r, mring_s, mring_r
        )
        common[...] = out[rows:S, :]
        b0[...] = dot(spread(True), out[0:rows, :].astype(BF)).astype(BF).reshape(NZ, NX, CAPP, H)
        for d in range(1, NZ):
            begin(send(b0.at[(z + d) % NZ], b1r.at[z], b1_s.at[d - 1], b1_rs.at[d - 1], at_z(d)))
        b1r[z] = b0[z]
        yield
        for d in range(1, NZ):
            send(b0.at[z], b1r.at[(z - d + NZ) % NZ], b1_s.at[d - 1], b1_rs.at[d - 1], at_z(d)).wait_recv()
        for d in range(1, NX):
            begin(send(b1r.at[:, (x + d) % NX], b2r.at[x], b2_s.at[d - 1], b2_rs.at[d - 1], at_x(d)))
        b2r[x] = b1r[:, x]
        yield
        for d in range(1, NX):
            send(b1r.at[:, x], b2r.at[(x - d + NX) % NX], b2_s.at[d - 1], b2_rs.at[d - 1], at_x(d)).wait_recv()
        gates = gated[...].T
        high = gates.astype(BF)
        low = (gates - high.astype(F32)).astype(BF)
        got = b2r[...].reshape(slots, H)
        mix[...] = (common[...] + dot(high, got) + dot(low, got)).astype(BF)

    attn, moe = attention(), experts()
    for turn in "mamamaamaamamamaamamaamamamama":
        next(attn if turn == "a" else moe, None)

    for when, copy in pending:
        if when is None:
            copy.wait_send()
        else:
            pl.when(when)(copy.wait_send)


def body(
    queries, keys, values, key_bias, out_weight, moe_input, moe_gain, route_ids, route_scores,
    shared_gate, shared_up, shared_down, expert_gate, expert_up, expert_down,
):
    hbm, vmem = pl.BlockSpec(memory_space=pl.ANY), pl.BlockSpec(memory_space=pltpu.VMEM)
    dma = pltpu.SemaphoreType.DMA
    V = pltpu.VMEM
    slots = (NZ, NX, CAPP, H)
    rs = [V((2, NY, S, H), BF), V((NY, S, H), BF), V((2, 4, S, H), BF), V((2, 4, S, H), BF)]
    sems = [dma((15,)), dma((3,)), dma((3,)), dma((2, 4, 2)), dma((2, 4, 2)), dma((3,)), dma((3,)), dma((7,)), dma((7,))]
    sems += [dma((2, 4)), dma((2, 4)), dma((8,)), dma((8,))]
    sems += [dma((7,)), dma((7,)), dma((3,)), dma((3,)), dma((3,)), dma((3,)), dma((3,)), dma((3,))]
    sems += [dma((8,)), dma((8,)), dma((2, 4, 2)), dma((2, 4, 2))] * 2
    return pl.pallas_call(
        kernel,
        out_shape=(jax.ShapeDtypeStruct((S, H), BF), jax.ShapeDtypeStruct((128, H), BF)),
        in_specs=[hbm] * 15,
        out_specs=(vmem, vmem),
        scratch_shapes=[
            V((NX * S, H), BF), V((NZ, KVR, H), BF), V((NZ, NX * S, H), F32), V((NX * S, H), F32),
            V((NX, NX, NZ, S), F32), V((NX, NZ, S), F32), V((NX - 1, S, H), BF), V((NX - 1, S, H), BF),
            V((S, H), F32), V((S, H), BF),
            V((1, S), BF), V((1, 2048), F32), V((2, 128), jnp.int32), V((2, 128), F32),
            V((2048, 2 * H), BF), V((2048, 2 * H), BF), V((H, 2048), BF), V((H, 2048), BF), V((H, 2048), BF),
            V((128, 2048), BF), V((128, 2048), BF), V((512, 128), F32),
            V((NX, NZ, CAPP, 2 * H), BF), V((NX, NZ, CAPP, 2 * H), BF), V((NZ, NX, CAPP, 2 * H), BF), V((16, NZ * NX * CAP, H), BF),
            V(slots, BF), V(slots, BF), V((NX, NZ, CAPP, H), BF), V((128, H), F32),
            *rs, *rs, *sems,
        ],
        compiler_params=pltpu.CompilerParams(
            collective_id=0, has_side_effects=True, vmem_limit_bytes=60 * 2**20
        ),
        name="fused",
    )(
        queries, keys, values, key_bias.T, out_weight, moe_input, moe_gain.reshape(1, -1), route_ids.T, route_scores.T,
        shared_gate, shared_up, shared_down,
        expert_gate.reshape(2048, H), expert_up.reshape(2048, H), expert_down.reshape(H, 2048),
    )


def solution(mesh):
    return jax.shard_map(
        body,
        mesh=mesh,
        in_specs=(
            P("ep", "tp"), P("ep", "tp"), P("ep", "tp"), P("ep", "tp"), P("tp", None), P("ep", None), P(),
            P("ep", None), P("ep", None), P(None, "tp"), P(None, "tp"), P("tp", None),
            P("ep", None, "tp"), P("ep", None, "tp"), P("ep", "tp", None),
        ),
        out_specs=(P("ep", "tp"), P("ep", "tp")),
        check_vma=False,
    )
```

time: 102 us -> 92.1 us (0.903)
  Pallas kernels: 95.1 us -> 88.5 us
  local copies, waits for them, and re-layouts: 4.81 us -> 2.19 us
    pallas_call x1, Pallas kernels: 95.1 us -> 88.5 us  [body(): pl.pallas_call(kernel, out_shape=(jax.ShapeDtypeStruct((S, H), BF), jax.S...]
    pad x3 -> x0, local copies, waits for them, and re-layouts: 1.79 us -> none  [the longest x1 0.6 us: body(): jnp.pad(key_bias.reshape(S // H, H), ((0, KVR - 2 * S - S // H), (0, 0)))]
    unnamed x10 -> x4, local copies, waits for them, and re-layouts: 3.03 us -> 2.19 us
where the time goes in v2:
time: 92.1 us; the launch traced here: 91.4 us
  Pallas kernels  88.5 us (96%)
  local copies, waits for them, and re-layouts  2.19 us (2%)
    pallas_call x1, Pallas kernels, body(): pl.pallas_call(kernel, out_shape=(jax.ShapeDtypeStruct((S, H), BF), jax.S...  88.5 us
    unnamed x4, local copies, waits for them, and re-layouts  2.19 us

profile of v2, /device:TPU:6, one launch (start us, length us, event | category | flops | bytes accessed | tf_op | source)
XLA Modules:
  0.0 91.4 jit_solution(6939680484932623042)
XLA Ops:
  0.6 88.5 %fused.1 = (bf16[512,128]{1,0:T(8,128)(2,1)}, bf16[128,128]{1,0:T(8,128)(2,1)}) custom-call(bf16[512,128]{1,0:T(8,128)(2,1)} %q_in.1, bf16[512,128]{1,0:T(8,128)(2,1)} %k_in.1, bf16[512,128]{1,0:T(8,128)(2,1)} %v_in.1, bf16[1,512]{1,0:T(2,128)(2,1)} %bitcast.11, bf16[128,2048]{1,0:T(8,128)(2,1)} %ow_in.1, bf16[128,2048]{1,0:T(8,128)(2,1)} %mi_in.1, ...), custom_call_target="tpu_custom_call" | custom-call | tf_op jit(solution)/shard_map/fused/pallas_call | solution.py:460
  89.2 0.0 copy-start
  89.2 1.6 %copy.19 = bf16[512,128]{1,0:T(8,128)(2,1)} copy(bf16[512,128]{1,0:T(8,128)(2,1)} %get-tuple-element.4) | data formatting | bytes 262144
  90.8 0.0 copy-done
  90.8 0.6 copy.20
Async XLA Ops:
  89.2 1.6 %copy-start = (bf16[128,128]{1,0:T(8,128)(2,1)S(1)}, bf16[128,128]{1,0:T(8,128)(2,1)}, u32[]{:S(2)}) copy-start(bf16[128,128]{1,0:T(8,128)(2,1)} %get-tuple-element.5) | copy-start | bytes 98308

commit v3 on v2

--- a/solution.py
+++ b/solution.py
@@ -11,7 +11,10 @@
 BF = jnp.bfloat16
 F32 = jnp.float32
 NX, NZ, NY = 4, 8, 8
-UP, DOWN = 4, 3
+UP = 4
+HELP = 3
+SHIFT = UP + 1
+BAND = 16
 LOG2E = 1.4426950408889634
 EPS_NORM = 1e-06
 ROUTED_SCALE = 2.5
@@ -55,11 +58,11 @@
 def kernel(
     q_in, k_in, v_in, bias_in, ow_in, mi_in, gain_in, ids_in, scores_in, sg_in, su_in, sd_in, eg_in, eu_in, ed_in,
     mixed, mix,
-    qb, kvb, op, tcol, tr, ts, osend, orecv, oacc, heads,
+    qb, kvb, op, tcol, tr, ts, osend, orecv, hsend, hrecv, oacc, factor, heads,
     bias, gain, ids, scores, wgu, sgu, ed, sd, ow, mi, normed, gated,
     a1s, a1r, a2r, ag, b0, b1r, b2r, common,
     part_m, sib_m, ring_m, rsend_m, part_a, sib_a, ring_a, rsend_a,
-    lsem, q_s, q_r, kv_s, kv_r, a1_s, a1_rs, a2_s, a2_rs, ag_s, ag_r, ags_s, ags_r,
+    lsem, q_s, q_r, qh_s, qh_r, h_s, h_r, kv_s, kv_r, a1_s, a1_rs, a2_s, a2_rs, ag_s, ag_r, ags_s, ags_r,
     b1_s, b1_rs, b2_s, b2_rs, t_s, t_r, o_s, o_r,
     msib_s, msib_r, mring_s, mring_r, asib_s, asib_r, aring_s, aring_r,
 ):
@@ -75,6 +78,9 @@
     def at_y(d):
         return {"ep": ep, "tp": ((y + d) % NY) * 2 + c}
 
+    opposite = {"ep": (NZ - 1 - z) * NX + x, "tp": tp}
+
+    helper, helped = z < HELP, z >= NZ - HELP
     sibling = {"ep": ep, "tp": y * 2 + (1 - c)}
 
     def send(src, dst, ssem, rsem, dev):
@@ -83,7 +89,7 @@
         )
 
     local = [
-        (q_in, qb.at[pl.ds(pl.multiple_of(x * S, S), S)]),
+        (q_in, qb.at[0, pl.ds(pl.multiple_of(x * S, S), S)]),
         (k_in, kvb.at[z, 0:S]),
         (v_in, kvb.at[z, KB:KVR]),
         (bias_in, bias),
@@ -120,8 +126,11 @@
 
     halves = (slice(0, KB), slice(KB, KVR))
 
-    def query_rows(i):
-        return qb.at[pl.ds(pl.multiple_of(i * S, S), S)]
+    def query_rows(i, which=0):
+        return qb.at[which, pl.ds(pl.multiple_of(i * S, S), S)]
+
+    def to_helper():
+        return send(query_rows(x), query_rows(x, 1), qh_s.at[0], qh_r.at[0], opposite)
 
     def up(d, h):
         block = kvb.at[jnp.maximum(z - d + 1, 0), halves[h]]
@@ -132,39 +141,47 @@
         return send(block, block, kv_s.at[0, d - 1, h], kv_r.at[0, d - 1, h], at_z(1))
 
     def down(d, h):
-        block = kvb.at[(z + d - 1) % NZ, halves[h]]
+        block = kvb.at[jnp.minimum(z + d - 1, NZ - 1), halves[h]]
         return send(block, block, kv_s.at[1, d - 1, h], kv_r.at[1, d - 1, h], at_z(-1))
 
     def down_arrival(d, h):
-        block = kvb.at[(z + d) % NZ, halves[h]]
+        block = kvb.at[jnp.minimum(z + d, NZ - 1), halves[h]]
         return send(block, block, kv_s.at[1, d - 1, h], kv_r.at[1, d - 1, h], at_z(-1))
 
-    def step(zi, first):
+    def step(which, zi, place, first):
         rows = kvb[zi, S:KB, :].astype(F32) * LOG2E
         row = jnp.concatenate([rows[j : j + 1, :] for j in range(S // H)], axis=1)
-        out, total = attend(qb[...], kvb[zi, 0:S, :], kvb[zi, KB:KVR, :], row, first)
-        op[zi] = out
-        tcol[...] = jnp.where(iota((NX * S, H), 1) == zi, total, tcol[...])
+        out, total = attend(qb[which], kvb[zi, 0:S, :], kvb[zi, KB:KVR, :], row, first)
+        op[place] = out
+        tcol[...] = jnp.where(iota((NX * S, H), 1) == place, total, tcol[...])
 
     def attention():
         fetch[0].wait()
         for d in range(1, NX):
             begin(send(query_rows(x), query_rows(x), q_s.at[d - 1], q_r.at[d - 1], at_x(d)))
         fetch[1].wait()
+        sends_down = (z >= 1) & (z < HELP)
         begin(up(1, 0), z < NZ - 1)
-        begin(down(1, 0), z < DOWN)
-        yield
+        begin(down(1, 0), sends_down)
         fetch[2].wait()
         begin(up(1, 1), z < NZ - 1)
-        begin(down(1, 1), z < DOWN)
+        begin(down(1, 1), sends_down)
+        begin(to_helper(), helped)
+        yield
         tcol[...] = jnp.zeros_like(tcol)
         for d in range(1, NX):
             src = query_rows((x - d + NX) % NX)
             send(src, src, q_s.at[d - 1], q_r.at[d - 1], at_x(d)).wait_recv()
-        step(z, x * S)
+
+        @pl.when(helper)
+        def _():
+            to_helper().wait_recv()
+
+        for d in range(1, NX):
+            begin(send(query_rows(x, 1), query_rows(x, 1), qh_s.at[d], qh_r.at[d], at_x(d)), helper)
+        step(0, z, 0, x * S)
         yield
         for d in range(1, UP + 1):
-            came = (z + d) % NZ
             for h in range(2):
 
                 @pl.when(z >= d)
@@ -173,27 +190,31 @@
 
                 if d < UP:
                     begin(up(d + 1, h), (z >= d) & (z < NZ - 1))
-                if d <= DOWN:
-
-                    @pl.when(came < DOWN)
+                if d < HELP:
+
+                    @pl.when(z < HELP - d)
                     def _():
                         down_arrival(d, h).wait_recv()
 
-                    if d < DOWN:
-                        begin(down(d + 1, h), came < DOWN)
-
-            @pl.when(z >= d)
+                    if d == 1:
+                        begin(down(2, h), z == 1)
+            if d == 2:
+
+                @pl.when(helper)
+                def _():
+                    for i in range(1, NX):
+                        src = query_rows((x - i + NX) % NX, 1)
+                        send(src, src, qh_s.at[i], qh_r.at[i], at_x(i)).wait_recv()
+
+            mine = z >= d
+            older = jnp.maximum(d - z - 2, 0)
+            zi = jnp.where(mine, z - d, older)
+
+            @pl.when(mine | ((d >= z + 2) & (d <= HELP + 1)))
             def _():
-                step(jnp.maximum(z - d, 0), None)
+                step(jnp.where(mine, 0, 1), zi, jnp.where(mine, d, SHIFT + older), None)
 
             yield
-            if d <= DOWN:
-
-                @pl.when((came < DOWN) & (came < z))
-                def _():
-                    step(came, None)
-
-                yield
         for qi in range(NX):
             ts[qi] = tcol[qi * S : (qi + 1) * S].T[0:NZ, :]
         for d in range(1, NX):
@@ -204,42 +225,109 @@
             src = tr.at[(x - d + NX) % NX]
             send(ts, src, t_s.at[d - 1], t_r.at[d - 1], at_x(d)).wait_recv()
 
-        def combine(qi):
+        def scales(qi):
             sums = [tr[i, qi] for i in range(NX)]
             row = sums[0] + sums[1] + sums[2] + sums[3]
             within = sum(jnp.where(i > x, sums[i], 0.0) for i in range(1, NX))
-            parts, run = [], jnp.zeros((1, S), F32)
-            for zi in reversed(range(NZ)):
-                parts.append(run)
-                run = run + row[zi : zi + 1, :]
-            carried = jnp.concatenate(parts[::-1], axis=0) + within
-            scale = jnp.exp2(-carried)
-            scale = jnp.concatenate([scale, jnp.zeros((H - NZ, S), F32)], axis=0).T
-            rows = pl.ds(pl.multiple_of(qi * S, S), S)
-            oacc[...] = scale[:, 0:1] * op[0, rows, :]
-            for zi in range(1, NZ):
-
-                @pl.when(zi <= z)
+            parts, nothing = [None] * NZ, jnp.zeros((1, S), F32)
+            run = nothing
+            for k in range(SHIFT):
+                parts[k] = run
+                run = run + row[k : k + 1, :]
+            after = nothing
+            for k in reversed(range(SHIFT, NZ)):
+                parts[k] = after
+                after = after + row[k : k + 1, :]
+            carried = jnp.concatenate(parts, axis=0) + within
+            return [jnp.exp2(-carried), jnp.exp2(-run), jnp.zeros((BAND - NZ - 1, S), F32)]
+
+        order = (1, 2, 3, 0)
+        bands = [part for d in order for part in scales((x + d) % NX)]
+        bands.append(jnp.zeros((H - NX * BAND, S), F32))
+        scale = jnp.concatenate(bands, axis=0).T
+
+        def share(j, k, rows):
+            return scale[:, j * BAND + k : j * BAND + k + 1] * op[k, rows, :]
+
+        def combine(j, rows):
+            @pl.when(z >= UP)
+            def _():
+                total = share(j, 0, rows)
+                for k in range(1, UP + 1):
+                    total = total + share(j, k, rows)
+                oacc[...] = total
+
+            @pl.when(z < UP)
+            def _():
+                oacc[...] = share(j, 0, rows)
+                for k in range(1, UP):
+
+                    @pl.when(k <= z)
+                    def _():
+                        oacc[...] += share(j, k, rows)
+
+        def combine_helped(j, d, rows):
+            @pl.when(helper)
+            def _():
+                oacc[...] = share(j, SHIFT, rows)
+                for i in range(1, HELP):
+
+                    @pl.when(i < HELP - z)
+                    def _():
+                        oacc[...] += share(j, SHIFT + i, rows)
+
+                if d > 0:
+                    hsend[d - 1] = oacc[...].astype(BF)
+                else:
+                    factor[...] = oacc[...]
+
+            if d > 0:
+                begin(help_out(d), helper)
+
+        def help_out(d):
+            return send(hsend.at[d - 1], hrecv.at[d - 1], h_s.at[d], h_r.at[d], at_x(d))
+
+        def help_home():
+            return send(hsend.at[NX - 1], hrecv.at[NX - 1], h_s.at[0], h_r.at[0], opposite)
+
+        for j, d in enumerate(order):
+            rows = pl.ds(pl.multiple_of(((x + d) % NX) * S, S), S)
+            combine_helped(j, d, rows)
+            combine(j, rows)
+            if d > 0:
+                osend[d - 1] = oacc[...].astype(BF)
+                begin(send(osend.at[d - 1], orecv.at[d - 1], o_s.at[d - 1], o_r.at[d - 1], at_x(d)))
+            else:
+                heads[...] = oacc[...]
+
+                @pl.when(helped)
                 def _():
-                    oacc[...] += scale[:, zi : zi + 1] * op[zi, rows, :]
-
-        for d in range(1, NX):
-            qi = (x + d) % NX
-            combine(qi)
-            osend[d - 1] = oacc[...].astype(BF)
-            begin(send(osend.at[d - 1], orecv.at[d - 1], o_s.at[d - 1], o_r.at[d - 1], at_x(d)))
-        combine(x)
-        yield
+                    factor[...] = jnp.broadcast_to(scale[:, j * BAND + NZ : j * BAND + NZ + 1], (S, H))
+
+        yield
+
+        @pl.when(helper)
+        def _():
+            for d in range(1, NX):
+                help_out(d).wait_recv()
+            far = factor[...] + hrecv[0].astype(F32) + hrecv[1].astype(F32) + hrecv[2].astype(F32)
+            hsend[NX - 1] = far.astype(BF)
+
+        begin(help_home(), helper)
         for d in range(1, NX):
             send(osend.at[d - 1], orecv.at[d - 1], o_s.at[d - 1], o_r.at[d - 1], at_x(d)).wait_recv()
-        total = oacc[...]
-        for d in range(1, NX):
-            total = total + orecv[d - 1].astype(F32)
-        heads[...] = total.astype(BF)
+        heads[...] += orecv[0].astype(F32) + orecv[1].astype(F32) + orecv[2].astype(F32)
+
+        @pl.when(helped)
+        def _():
+            help_home().wait_recv()
+            heads[...] += factor[...] * hrecv[NX - 1].astype(F32)
+
+        rounded = heads[...].astype(BF)
         fetch[11].wait()
 
         def fill(yi):
-            both = dot(heads[...], ow[:, pl.ds(pl.multiple_of(yi * 256, 256), 256)]).astype(BF)
+            both = dot(rounded, ow[:, pl.ds(pl.multiple_of(yi * 256, 256), 256)]).astype(BF)
             part_a[0, yi] = both[:, :H]
             part_a[1, yi] = both[:, H:]
 
@@ -411,7 +499,7 @@
             part_m[1, yi, rows:S] = both[:, H:]
 
         out = yield from reduce_scatter(
-            fill, 1, part_m, sib_m, ring_m, rsend_m, msib_s, msib_r, mring_s, mring_r
+            fill, 2, part_m, sib_m, ring_m, rsend_m, msib_s, msib_r, mring_s, mring_r
         )
         common[...] = out[rows:S, :]
         b0[...] = dot(spread(True), out[0:rows, :].astype(BF)).astype(BF).reshape(NZ, NX, CAPP, H)
@@ -434,7 +522,7 @@
         mix[...] = (common[...] + dot(high, got) + dot(low, got)).astype(BF)
 
     attn, moe = attention(), experts()
-    for turn in "mamamaamaamamamaamamaamamamama":
+    for turn in "mamamamamamamaamamamamaamam":
         next(attn if turn == "a" else moe, None)
 
     for when, copy in pending:
@@ -453,7 +541,7 @@
     V = pltpu.VMEM
     slots = (NZ, NX, CAPP, H)
     rs = [V((2, NY, S, H), BF), V((NY, S, H), BF), V((2, 4, S, H), BF), V((2, 4, S, H), BF)]
-    sems = [dma((15,)), dma((3,)), dma((3,)), dma((2, 4, 2)), dma((2, 4, 2)), dma((3,)), dma((3,)), dma((7,)), dma((7,))]
+    sems = [dma((15,)), dma((3,)), dma((3,)), dma((4,)), dma((4,)), dma((4,)), dma((4,)), dma((2, 4, 2)), dma((2, 4, 2)), dma((3,)), dma((3,)), dma((7,)), dma((7,))]
     sems += [dma((2, 4)), dma((2, 4)), dma((8,)), dma((8,))]
     sems += [dma((7,)), dma((7,)), dma((3,)), dma((3,)), dma((3,)), dma((3,)), dma((3,)), dma((3,))]
     sems += [dma((8,)), dma((8,)), dma((2, 4, 2)), dma((2, 4, 2))] * 2
@@ -463,9 +551,9 @@
         in_specs=[hbm] * 15,
         out_specs=(vmem, vmem),
         scratch_shapes=[
-            V((NX * S, H), BF), V((NZ, KVR, H), BF), V((NZ, NX * S, H), F32), V((NX * S, H), F32),
+            V((2, NX * S, H), BF), V((NZ, KVR, H), BF), V((NZ, NX * S, H), F32), V((NX * S, H), F32),
             V((NX, NX, NZ, S), F32), V((NX, NZ, S), F32), V((NX - 1, S, H), BF), V((NX - 1, S, H), BF),
-            V((S, H), F32), V((S, H), BF),
+            V((NX, S, H), BF), V((NX, S, H), BF), V((S, H), F32), V((S, H), F32), V((S, H), F32),
             V((1, S), BF), V((1, 2048), F32), V((2, 128), jnp.int32), V((2, 128), F32),
             V((2048, 2 * H), BF), V((2048, 2 * H), BF), V((H, 2048), BF), V((H, 2048), BF), V((H, 2048), BF),
             V((128, 2048), BF), V((128, 2048), BF), V((512, 128), F32),

time: 92.1 us -> 98.5 us (1.069)
  Pallas kernels: 88.5 us -> 95 us
    pallas_call x1, Pallas kernels: 88.5 us -> 95 us  [body(): pl.pallas_call(kernel, out_shape=(jax.ShapeDtypeStruct((S, H), BF), jax.S...]
where the time goes in v3:
time: 98.5 us; the launch traced here: 97.9 us
  Pallas kernels  95 us (96%)
  local copies, waits for them, and re-layouts  2.19 us (2%)
    pallas_call x1, Pallas kernels, body(): pl.pallas_call(kernel, out_shape=(jax.ShapeDtypeStruct((S, H), BF), jax.S...  95 us
    unnamed x4, local copies, waits for them, and re-layouts  2.19 us

profile of v3, /device:TPU:6, one launch (start us, length us, event | category | flops | bytes accessed | tf_op | source)
XLA Modules:
  0.0 97.9 jit_solution(17256919919927028237)
XLA Ops:
  0.6 95.0 %fused.1 = (bf16[512,128]{1,0:T(8,128)(2,1)}, bf16[128,128]{1,0:T(8,128)(2,1)}) custom-call(bf16[512,128]{1,0:T(8,128)(2,1)} %q_in.1, bf16[512,128]{1,0:T(8,128)(2,1)} %k_in.1, bf16[512,128]{1,0:T(8,128)(2,1)} %v_in.1, bf16[1,512]{1,0:T(2,128)(2,1)} %bitcast.11, bf16[128,2048]{1,0:T(8,128)(2,1)} %ow_in.1, bf16[128,2048]{1,0:T(8,128)(2,1)} %mi_in.1, ...), custom_call_target="tpu_custom_call" | custom-call | tf_op jit(solution)/shard_map/fused/pallas_call | solution.py:548
  95.7 0.0 copy-start
  95.7 1.6 %copy.19 = bf16[512,128]{1,0:T(8,128)(2,1)} copy(bf16[512,128]{1,0:T(8,128)(2,1)} %get-tuple-element.4) | data formatting | bytes 262144
  97.3 0.0 copy-done
  97.3 0.6 copy.20
Async XLA Ops:
  95.7 1.6 %copy-start = (bf16[128,128]{1,0:T(8,128)(2,1)S(1)}, bf16[128,128]{1,0:T(8,128)(2,1)}, u32[]{:S(2)}) copy-start(bf16[128,128]{1,0:T(8,128)(2,1)} %get-tuple-element.5) | copy-start | bytes 98308

commit v4 on v3

--- a/solution.py
+++ b/solution.py
@@ -58,12 +58,12 @@
 def kernel(
     q_in, k_in, v_in, bias_in, ow_in, mi_in, gain_in, ids_in, scores_in, sg_in, su_in, sd_in, eg_in, eu_in, ed_in,
     mixed, mix,
-    qb, kvb, op, tcol, tr, ts, osend, orecv, hsend, hrecv, oacc, factor, heads,
+    qb, kvb, op, tcol, tr, ts, tr2, ts2, osend, orecv, hsend, hrecv, oacc, factor, heads,
     bias, gain, ids, scores, wgu, sgu, ed, sd, ow, mi, normed, gated,
     a1s, a1r, a2r, ag, b0, b1r, b2r, common,
     part_m, sib_m, ring_m, rsend_m, part_a, sib_a, ring_a, rsend_a,
     lsem, q_s, q_r, qh_s, qh_r, h_s, h_r, kv_s, kv_r, a1_s, a1_rs, a2_s, a2_rs, ag_s, ag_r, ags_s, ags_r,
-    b1_s, b1_rs, b2_s, b2_rs, t_s, t_r, o_s, o_r,
+    b1_s, b1_rs, b2_s, b2_rs, t_s, t_r, t2_s, t2_r, o_s, o_r,
     msib_s, msib_r, mring_s, mring_r, asib_s, asib_r, aring_s, aring_r,
 ):
     ep, tp = lax.axis_index("ep"), lax.axis_index("tp")
@@ -181,6 +181,9 @@
             begin(send(query_rows(x, 1), query_rows(x, 1), qh_s.at[d], qh_r.at[d], at_x(d)), helper)
         step(0, z, 0, x * S)
         yield
+        def sums_of(qi):
+            return tcol[qi * S : (qi + 1) * S].T[0:NZ, :]
+
         for d in range(1, UP + 1):
             for h in range(2):
 
@@ -190,43 +193,52 @@
 
                 if d < UP:
                     begin(up(d + 1, h), (z >= d) & (z < NZ - 1))
-                if d < HELP:
-
-                    @pl.when(z < HELP - d)
+                if d == 1 or d == HELP:
+                    hops = 1 if d == 1 else HELP - 1
+
+                    @pl.when(z < HELP - hops)
                     def _():
-                        down_arrival(d, h).wait_recv()
+                        down_arrival(hops, h).wait_recv()
 
                     if d == 1:
                         begin(down(2, h), z == 1)
-            if d == 2:
-
-                @pl.when(helper)
+            if d <= HELP:
+
+                @pl.when(z == d - 1)
                 def _():
                     for i in range(1, NX):
                         src = query_rows((x - i + NX) % NX, 1)
                         send(src, src, qh_s.at[i], qh_r.at[i], at_x(i)).wait_recv()
 
             mine = z >= d
-            older = jnp.maximum(d - z - 2, 0)
+            older = jnp.maximum(d - z - 1, 0)
             zi = jnp.where(mine, z - d, older)
 
-            @pl.when(mine | ((d >= z + 2) & (d <= HELP + 1)))
+            @pl.when(mine | (d <= HELP))
             def _():
                 step(jnp.where(mine, 0, 1), zi, jnp.where(mine, d, SHIFT + older), None)
 
+            if d == UP - 1:
+                for qi in range(NX):
+                    ts[qi] = sums_of(qi)
+                for i in range(1, NX):
+                    begin(send(ts, tr.at[x], t_s.at[i - 1], t_r.at[i - 1], at_x(i)))
+                tr[x] = ts[...]
             yield
+        newest = iota((NZ, S), 0) == UP
         for qi in range(NX):
-            ts[qi] = tcol[qi * S : (qi + 1) * S].T[0:NZ, :]
-        for d in range(1, NX):
-            begin(send(ts, tr.at[x], t_s.at[d - 1], t_r.at[d - 1], at_x(d)))
-        tr[x] = ts[...]
-        yield
-        for d in range(1, NX):
-            src = tr.at[(x - d + NX) % NX]
+            ts2[qi] = jnp.sum(jnp.where(newest, sums_of(qi), 0.0), axis=0, keepdims=True)
+        for d in range(1, NX):
+            begin(send(ts2, tr2.at[x], t2_s.at[d - 1], t2_r.at[d - 1], at_x(d)))
+        tr2[x] = ts2[...]
+        yield
+        for d in range(1, NX):
+            src, src2 = tr.at[(x - d + NX) % NX], tr2.at[(x - d + NX) % NX]
             send(ts, src, t_s.at[d - 1], t_r.at[d - 1], at_x(d)).wait_recv()
+            send(ts2, src2, t2_s.at[d - 1], t2_r.at[d - 1], at_x(d)).wait_recv()
 
         def scales(qi):
-            sums = [tr[i, qi] for i in range(NX)]
+            sums = [tr[i, qi] + jnp.where(newest, tr2[i, qi], 0.0) for i in range(NX)]
             row = sums[0] + sums[1] + sums[2] + sums[3]
             within = sum(jnp.where(i > x, sums[i], 0.0) for i in range(1, NX))
             parts, nothing = [None] * NZ, jnp.zeros((1, S), F32)
@@ -291,9 +303,9 @@
             return send(hsend.at[NX - 1], hrecv.at[NX - 1], h_s.at[0], h_r.at[0], opposite)
 
         for j, d in enumerate(order):
-            rows = pl.ds(pl.multiple_of(((x + d) % NX) * S, S), S)
-            combine_helped(j, d, rows)
-            combine(j, rows)
+            combine_helped(j, d, pl.ds(pl.multiple_of(((x + d) % NX) * S, S), S))
+        for j, d in enumerate(order):
+            combine(j, pl.ds(pl.multiple_of(((x + d) % NX) * S, S), S))
             if d > 0:
                 osend[d - 1] = oacc[...].astype(BF)
                 begin(send(osend.at[d - 1], orecv.at[d - 1], o_s.at[d - 1], o_r.at[d - 1], at_x(d)))
@@ -314,6 +326,7 @@
             hsend[NX - 1] = far.astype(BF)
 
         begin(help_home(), helper)
+        yield
         for d in range(1, NX):
             send(osend.at[d - 1], orecv.at[d - 1], o_s.at[d - 1], o_r.at[d - 1], at_x(d)).wait_recv()
         heads[...] += orecv[0].astype(F32) + orecv[1].astype(F32) + orecv[2].astype(F32)
@@ -332,7 +345,7 @@
             part_a[1, yi] = both[:, H:]
 
         out = yield from reduce_scatter(
-            fill, 2, part_a, sib_a, ring_a, rsend_a, asib_s, asib_r, aring_s, aring_r
+            fill, 4, part_a, sib_a, ring_a, rsend_a, asib_s, asib_r, aring_s, aring_r
         )
         mixed[...] = out.astype(BF)
 
@@ -522,7 +535,7 @@
         mix[...] = (common[...] + dot(high, got) + dot(low, got)).astype(BF)
 
     attn, moe = attention(), experts()
-    for turn in "mamamamamamamaamamamamaamam":
+    for turn in "mamamaamammamaamamamamaamama":
         next(attn if turn == "a" else moe, None)
 
     for when, copy in pending:
@@ -543,8 +556,8 @@
     rs = [V((2, NY, S, H), BF), V((NY, S, H), BF), V((2, 4, S, H), BF), V((2, 4, S, H), BF)]
     sems = [dma((15,)), dma((3,)), dma((3,)), dma((4,)), dma((4,)), dma((4,)), dma((4,)), dma((2, 4, 2)), dma((2, 4, 2)), dma((3,)), dma((3,)), dma((7,)), dma((7,))]
     sems += [dma((2, 4)), dma((2, 4)), dma((8,)), dma((8,))]
-    sems += [dma((7,)), dma((7,)), dma((3,)), dma((3,)), dma((3,)), dma((3,)), dma((3,)), dma((3,))]
-    sems += [dma((8,)), dma((8,)), dma((2, 4, 2)), dma((2, 4, 2))] * 2
+    sems += [dma((7,)), dma((7,)), dma((3,)), dma((3,)), dma((3,)), dma((3,)), dma((3,)), dma((3,)), dma((3,)), dma((3,))]
+    sems += [dma((8,)), dma((8,)), dma((2, 4, 4)), dma((2, 4, 4))] * 2
     return pl.pallas_call(
         kernel,
         out_shape=(jax.ShapeDtypeStruct((S, H), BF), jax.ShapeDtypeStruct((128, H), BF)),
@@ -552,7 +565,8 @@
         out_specs=(vmem, vmem),
         scratch_shapes=[
             V((2, NX * S, H), BF), V((NZ, KVR, H), BF), V((NZ, NX * S, H), F32), V((NX * S, H), F32),
-            V((NX, NX, NZ, S), F32), V((NX, NZ, S), F32), V((NX - 1, S, H), BF), V((NX - 1, S, H), BF),
+            V((NX, NX, NZ, S), F32), V((NX, NZ, S), F32), V((NX, NX, 1, S), F32), V((NX, 1, S), F32),
+            V((NX - 1, S, H), BF), V((NX - 1, S, H), BF),
             V((NX, S, H), BF), V((NX, S, H), BF), V((S, H), F32), V((S, H), F32), V((S, H), F32),
             V((1, S), BF), V((1, 2048), F32), V((2, 128), jnp.int32), V((2, 128), F32),
             V((2048, 2 * H), BF), V((2048, 2 * H), BF), V((H, 2048), BF), V((H, 2048), BF), V((H, 2048), BF),

time: 98.5 us -> 91.9 us (0.933)
  Pallas kernels: 95 us -> 88.6 us
    pallas_call x1, Pallas kernels: 95 us -> 88.6 us  [body(): pl.pallas_call(kernel, out_shape=(jax.ShapeDtypeStruct((S, H), BF), jax.S...]
where the time goes in v4:
time: 91.9 us; the launch traced here: 91.4 us
  Pallas kernels  88.6 us (96%)
  local copies, waits for them, and re-layouts  2.19 us (2%)
    pallas_call x1, Pallas kernels, body(): pl.pallas_call(kernel, out_shape=(jax.ShapeDtypeStruct((S, H), BF), jax.S...  88.6 us
    unnamed x4, local copies, waits for them, and re-layouts  2.19 us

profile of v4, /device:TPU:6, one launch (start us, length us, event | category | flops | bytes accessed | tf_op | source)
XLA Modules:
  0.0 91.4 jit_solution(9210379154739229297)
XLA Ops:
  0.6 88.6 %fused.1 = (bf16[512,128]{1,0:T(8,128)(2,1)}, bf16[128,128]{1,0:T(8,128)(2,1)}) custom-call(bf16[512,128]{1,0:T(8,128)(2,1)} %q_in.1, bf16[512,128]{1,0:T(8,128)(2,1)} %k_in.1, bf16[512,128]{1,0:T(8,128)(2,1)} %v_in.1, bf16[1,512]{1,0:T(2,128)(2,1)} %bitcast.11, bf16[128,2048]{1,0:T(8,128)(2,1)} %ow_in.1, bf16[128,2048]{1,0:T(8,128)(2,1)} %mi_in.1, ...), custom_call_target="tpu_custom_call" | custom-call | tf_op jit(solution)/shard_map/fused/pallas_call | solution.py:561
  89.2 0.0 copy-start
  89.2 1.6 %copy.19 = bf16[512,128]{1,0:T(8,128)(2,1)} copy(bf16[512,128]{1,0:T(8,128)(2,1)} %get-tuple-element.4) | data formatting | bytes 262144
  90.8 0.0 copy-done
  90.8 0.6 copy.20
Async XLA Ops:
  89.2 1.6 %copy-start = (bf16[128,128]{1,0:T(8,128)(2,1)S(1)}, bf16[128,128]{1,0:T(8,128)(2,1)}, u32[]{:S(2)}) copy-start(bf16[128,128]{1,0:T(8,128)(2,1)} %get-tuple-element.5) | copy-start | bytes 98308

commit v5 on v4

--- a/solution.py
+++ b/solution.py
@@ -535,7 +535,7 @@
         mix[...] = (common[...] + dot(high, got) + dot(low, got)).astype(BF)
 
     attn, moe = attention(), experts()
-    for turn in "mamamaamammamaamamamamaamama":
+    for turn in "mamamaamammamamamamaamaamama":
         next(attn if turn == "a" else moe, None)
 
     for when, copy in pending:

time: 91.9 us -> 92.3 us (level)
  the two profiles are of different devices: /device:TPU:6 before, /device:TPU:128 now
where the time goes in v5:
time: 92.3 us; the launch traced here: 92.1 us
  Pallas kernels  89.3 us (97%)
  local copies, waits for them, and re-layouts  2.19 us (2%)
    pallas_call x1, Pallas kernels, body(): pl.pallas_call(kernel, out_shape=(jax.ShapeDtypeStruct((S, H), BF), jax.S...  89.3 us
    unnamed x4, local copies, waits for them, and re-layouts  2.19 us

profile of v5, /device:TPU:128, one launch (start us, length us, event | category | flops | bytes accessed | tf_op | source)
XLA Modules:
  0.0 92.1 jit_solution(625016919744585167)
XLA Ops:
  0.6 89.3 %fused.1 = (bf16[512,128]{1,0:T(8,128)(2,1)}, bf16[128,128]{1,0:T(8,128)(2,1)}) custom-call(bf16[512,128]{1,0:T(8,128)(2,1)} %q_in.1, bf16[512,128]{1,0:T(8,128)(2,1)} %k_in.1, bf16[512,128]{1,0:T(8,128)(2,1)} %v_in.1, bf16[1,512]{1,0:T(2,128)(2,1)} %bitcast.11, bf16[128,2048]{1,0:T(8,128)(2,1)} %ow_in.1, bf16[128,2048]{1,0:T(8,128)(2,1)} %mi_in.1, ...), custom_call_target="tpu_custom_call" | custom-call | tf_op jit(solution)/shard_map/fused/pallas_call | solution.py:561
  89.9 0.0 copy-start
  89.9 1.6 %copy.19 = bf16[512,128]{1,0:T(8,128)(2,1)} copy(bf16[512,128]{1,0:T(8,128)(2,1)} %get-tuple-element.4) | data formatting | bytes 262144
  91.5 0.0 copy-done
  91.5 0.6 copy.20
Async XLA Ops:
  89.9 1.6 %copy-start = (bf16[128,128]{1,0:T(8,128)(2,1)S(1)}, bf16[128,128]{1,0:T(8,128)(2,1)}, u32[]{:S(2)}) copy-start(bf16[128,128]{1,0:T(8,128)(2,1)} %get-tuple-element.5) | copy-start | bytes 98308
